TPU v7x, 32 devices: a whole 2x2x4 slice. The times are simulated.
32 devices in a mesh: ep: 8 (over z, core), tp: 4 (over y, x).
Axes of the slice: x: 2, y: 2, z: 4, core: 2. Of those that a mesh axis runs over, the one named last changes fastest.
Arguments:
- tokens: bfloat16 [2048, 2048], P('ep'), may hold values from -6 to 6
- gate_proj: bfloat16 [8, 2048, 4096], P('ep', None, 'tp'), may hold values from -0.125 to 0.125
- up_proj: bfloat16 [8, 2048, 4096], P('ep', None, 'tp'), may hold values from -0.125 to 0.125
- down_proj: bfloat16 [8, 4096, 2048], P('ep', 'tp'), may hold values from -0.09375 to 0.09375
- side_input_weight: bfloat16 [2048, 1024], P(None, 'tp'), may hold values from -0.125 to 0.125
- dense_out: bfloat16 [1024, 2048], P(None, 'tp'), may hold values from -0.1875 to 0.1875
- dense_gate: bfloat16 [2048], replicated, may hold values from -0.125 to 0.125
- chosen_rows: int32 [8, 256], P(None, 'ep'), may hold values from 0 to 255, as said below
- choice_weights: float32 [8, 256], P(None, 'ep'), may hold values from 0.25 to 1
Outputs:
- mixed: bfloat16 [2048, 2048], P('ep', 'tp')
Inputs may be any that keep to these rules, and one draw needn't show every extreme that they name: `chosen_rows`: for each expert and each block of 32 columns (one index of ep), the 32 rows are distinct rows of that index's 256 tokens; every expert reads exactly 32 tokens of every index.
All inputs are finite; a program needn't handle non-finite values.
Results may differ from a plain program's by a relative error of at most 0.015.
Values may be sent and summed in bfloat16 or wider, within the bound.
No kernel may reach another device: no remote copies, remote signals or barrier semaphores. Data moves between devices by JAX's collectives and lax.ppermute only.
A program may use at most 64 MiB of HBM per device.

v0:
```python
import jax
import jax.numpy as jnp
from jax import lax
from jax.sharding import PartitionSpec as P


def per_device(
    tokens,
    gate_proj,
    up_proj,
    down_proj,
    side_input_weight,
    dense_out,
    dense_gate,
    chosen_rows,
    choice_weights,
):
    tok_rows = tokens.shape[0]
    width = tokens.shape[1] // lax.axis_size("tp")
    column_position = lax.axis_index("tp") * width
    own_cols = lax.dynamic_slice_in_dim(tokens, column_position, width, 1)
    expert_count, slot_rows = chosen_rows.shape
    capacity = expert_count * slot_rows
    picked = jnp.take(own_cols, chosen_rows.reshape(-1), axis=0).reshape(
        expert_count, slot_rows, width
    )
    arrived = lax.all_to_all(picked, "ep", split_axis=0, concat_axis=1, tiled=True).reshape(
        capacity, width
    )
    w_gate = gate_proj[0]
    w_up = up_proj[0]
    w_down = down_proj[0]
    piece = lax.all_gather(arrived, "tp", axis=1, tiled=True)
    gate_val = jnp.dot(piece, w_gate, preferred_element_type=jnp.float32)
    up_val = jnp.dot(piece, w_up, preferred_element_type=jnp.float32)
    hidden = (jax.nn.silu(gate_val) * up_val).astype(jnp.bfloat16)
    summed = lax.psum_scatter(
        lax.dot_general(
            w_down, hidden, (((0,), (1,)), ((), ())), preferred_element_type=jnp.float32
        ).astype(jnp.bfloat16),
        "tp",
        scatter_dimension=0,
        tiled=True,
    )
    returned = lax.all_to_all(summed, "ep", split_axis=1, concat_axis=1, tiled=True)
    hits = (
        chosen_rows.reshape(-1)[:, None] == jnp.arange(tok_rows, dtype=jnp.int32)[None, :]
    ).astype(jnp.bfloat16)
    scaled = returned.astype(jnp.float32) * choice_weights.reshape(-1)[None, :]
    high_part = scaled.astype(jnp.bfloat16)
    lower_half = (scaled - high_part.astype(jnp.float32)).astype(jnp.bfloat16)
    contract = (((0,), (1,)), ((), ()))
    routed = lax.dot_general(
        hits, high_part, contract, preferred_element_type=jnp.float32
    ) + lax.dot_general(hits, lower_half, contract, preferred_element_type=jnp.float32)
    dense_hidden = jax.nn.silu(
        jnp.dot(tokens, side_input_weight, preferred_element_type=jnp.float32)
    ).astype(jnp.bfloat16)
    dense_val = jnp.dot(
        lax.all_gather(dense_hidden, "tp", axis=1, tiled=True),
        dense_out,
        preferred_element_type=jnp.float32,
    )
    side_gate = jax.nn.sigmoid(jnp.dot(tokens, dense_gate, preferred_element_type=jnp.float32))
    return (routed + side_gate[:, None] * dense_val).astype(jnp.bfloat16)


def solution(mesh):
    placed = (
        P("ep", None),
        P("ep", None, "tp"),
        P("ep", None, "tp"),
        P("ep", "tp", None),
        P(None, "tp"),
        P(None, "tp"),
        P(),
        P(None, "ep"),
        P(None, "ep"),
    )
    return jax.shard_map(
        per_device, mesh=mesh, in_specs=placed, out_specs=P("ep", "tp"), check_vma=False
    )
```

profile of v0, /device:TPU:0, one launch (start us, length us, event | category | flops | bytes accessed | tf_op | source)
XLA Modules:
  0.0 116.5 jit_solution(18036005292770435474)
XLA Ops:
  6.5 0.0 copy-start
  6.5 0.0 all-gather.2.cloned.1.call-start
  6.5 0.9 reshape.57
  7.4 0.7 compare_and_fusion
  8.1 0.0 copy-done
  8.1 1.2 gather_fusion
  9.3 0.1 broadcast_select_fusion
  9.4 16.0 %all_to_all.18 = bf16[8,32,512]{2,1,0:T(8,128)(2,1)} all-to-all(bf16[8,32,512]{2,1,0:T(8,128)(2,1)S(1)} %broadcast_select_fusion), channel_id=1, replica_groups=mesh['ep'=8,'tp'=4] {'ep'}, dimensions={0} | all-to-all | bytes 524288 | tf_op jit(solution)/shard_map/all_to_all | solution.py:27
  25.4 0.0 all-gather.2.cloned.1.call-update
  25.4 0.0 reduce-scatter.2.cloned.1.call-start
  25.4 25.4 %all-gather.2.cloned.1.call-done = bf16[256,2048]{1,0:T(8,128)(2,1)} async-done(((bf16[256,512]{1,0:T(8,128)(2,1)}), bf16[256,2048]{1,0:T(8,128)(2,1)}) %all-gather.2.cloned.1.call-update) | async-done | bytes 1048592 | tf_op jit(solution)/shard_map/all_gather | solution.py:33
  50.9 0.0 copy-start.5
  50.9 3.8 %fusion.4 = f32[256,1024]{1,0:T(8,128)S(1)} fusion(bf16[256,2048]{1,0:T(8,128)(2,1)} %all-gather.2.cloned.1.call-done, bf16[1,2048,1024]{2,1,0:T(8,128)(2,1)} %param.10), kind=kOutput, calls=%fused_computation.5 | convolution fusion | flops 1073741824 | bytes 6291456 | tf_op jit(solution)/shard_map/dot_general | solution.py:34
  54.7 0.0 copy-done.5
  54.7 0.0 copy-start.2
  54.7 0.0 copy-start.4
  54.7 0.0 copy-start.3
  54.7 6.9 %fusion.9 = bf16[2048,256]{0,1:T(8,128)(2,1)} fusion(bf16[1,1024,2048]{2,1,0:T(8,128)(2,1)} %param.12, bf16[256,2048]{1,0:T(8,128)(2,1)S(1)} %copy-done.5, bf16[1,2048,1024]{2,1,0:T(8,128)(2,1)} %param.11, f32[256,1024]{1,0:T(8,128)S(1)} %fusion.4), kind=kOutput, calls=%fused_computation.8 | convolution fusion | flops 2149580800 | bytes 11534336 | tf_op jit(solution)/shard_map/dot_general | solution.py:38
  61.7 0.0 reduce-scatter.2.cloned.1.call-update
  61.7 0.0 copy-done.2
  61.7 0.1 eq.15
  61.8 0.0 copy-done.4
  61.8 0.1 mul.35
  61.8 0.0 copy-done.3
  61.9 0.0 copy-start.1
  61.9 1.8 %multiply_convert_fusion = bf16[256,256]{1,0:T(8,128)(2,1)S(1)} fusion(bf16[256,2048]{1,0:T(8,128)(2,1)S(1)} %copy-done, bf16[2048,256]{1,0:T(8,128)(2,1)} %param.13), kind=kOutput, calls=%fused_computation.20 | convolution fusion | flops 268763136 | bytes 2228224 | tf_op jit(solution)/shard_map/dot_general | solution.py:57
  63.6 17.9 %all_gather.7 = bf16[256,1024]{1,0:T(8,128)(2,1)S(1)} all-gather(bf16[256,256]{1,0:T(8,128)(2,1)S(1)} %multiply_convert_fusion), channel_id=1, replica_groups=mesh['ep'=8,'tp'=4] {'tp'}, dimensions={1}, use_global_device_ids=true | all-gather | bytes 655360 | tf_op jit(solution)/shard_map/all_gather | solution.py:60
  81.6 11.8 %reduce-scatter.2.cloned.1.call-done = bf16[512,256]{0,1:T(8,128)(2,1)} async-done(((bf16[2048,256]{0,1:T(8,128)(2,1)}), bf16[512,256]{0,1:T(8,128)(2,1)}) %reduce-scatter.2.cloned.1.call-update) | async-done | bytes 262160 | tf_op jit(solution)/shard_map/reduce_scatter | solution.py:37
  93.3 4.6 %all-to-all-start.1 = ((bf16[512,8,32]{0,2,1:T(8,128)(2,1)}), bf16[512,8,32]{0,2,1:T(8,128)(2,1)S(1)}, u32[]{:S(2)}, u32[]{:S(2)}) async-start(bf16[512,8,32]{0,2,1:T(8,128)(2,1)} %bitcast.41), calls=%async_computation.2 | async-start | bytes 524288 | tf_op jit(solution)/shard_map/all_to_all | solution.py:45
  97.9 0.4 fusion.32
  98.3 9.3 %all-to-all-done.1 = bf16[512,8,32]{0,2,1:T(8,128)(2,1)S(1)} async-done(((bf16[512,8,32]{0,2,1:T(8,128)(2,1)}), bf16[512,8,32]{0,2,1:T(8,128)(2,1)S(1)}, u32[]{:S(2)}, u32[]{:S(2)}) %all-to-all-start.1) | async-done | bytes 262176 | tf_op jit(solution)/shard_map/all_to_all | solution.py:45
  107.7 0.1 fusion.23
  107.8 0.3 fusion.28
  108.1 0.4 convolution_add_fusion
  108.5 0.0 copy-done.1
  108.5 1.1 fusion.19
  (5 shorter events, 0.1 us)
Async XLA Ops:
  6.5 1.6 %copy-start = (bf16[256,2048]{1,0:T(8,128)(2,1)S(1)}, bf16[256,2048]{1,0:T(8,128)(2,1)}, u32[]{:S(2)}) copy-start(bf16[256,2048]{1,0:T(8,128)(2,1)} %param.9) | copy-start | bytes 3145732
  6.5 44.3 %all-gather.2.cloned.1.call-start = ((), (), s32[]{:S(2)}) async-start(), calls=%async_computation.3 | async-start | bytes 1310720 | tf_op jit(solution)/shard_map/all_gather | solution.py:33
  25.4 67.9 %reduce-scatter.2.cloned.1.call-start = ((), (), s32[]{:S(2)}) async-start(), calls=%async_computation.4 | async-start | bytes 1310720 | tf_op jit(solution)/shard_map/reduce_scatter | solution.py:37
  50.9 3.8 %copy-start.5 = (bf16[256,2048]{1,0:T(8,128)(2,1)S(1)}, bf16[256,2048]{1,0:T(8,128)(2,1)}, u32[]{:S(2)}) copy-start(bf16[256,2048]{1,0:T(8,128)(2,1)} %all-gather.2.cloned.1.call-done) | copy-start | bytes 3145732
  54.7 7.0 %copy-start.2 = (s32[8,32]{1,0:T(8,128)S(1)}, s32[8,32]{1,0:T(8,128)}, u32[]{:S(2)}) copy-start(s32[8,32]{1,0:T(8,128)} %param.16) | copy-start | bytes 3076
  54.7 7.0 %copy-start.4 = (f32[8,32]{1,0:T(8,128)S(1)}, f32[8,32]{1,0:T(8,128)}, u32[]{:S(2)}) copy-start(f32[8,32]{1,0:T(8,128)} %param.17) | copy-start | bytes 3076
  54.7 7.1 %copy-start.3 = (bf16[2048]{0:T(1024)(128)(2,1)S(1)}, bf16[2048]{0:T(1024)(128)(2,1)}, u32[]{:S(2)}) copy-start(bf16[2048]{0:T(1024)(128)(2,1)} %param.15) | copy-start | bytes 12292
  61.9 46.7 %copy-start.1 = (bf16[1024,512]{1,0:T(8,128)(2,1)S(1)}, bf16[1024,512]{1,0:T(8,128)(2,1)}, u32[]{:S(2)}) copy-start(bf16[1024,512]{1,0:T(8,128)(2,1)} %param.14) | copy-start | bytes 3145732
  93.3 14.3 %all-to-all-start.1 = ((bf16[512,8,32]{0,2,1:T(8,128)(2,1)}), bf16[512,8,32]{0,2,1:T(8,128)(2,1)S(1)}, u32[]{:S(2)}, u32[]{:S(2)}) async-start(bf16[512,8,32]{0,2,1:T(8,128)(2,1)} %bitcast.41), calls=%async_computation.2 | async-start | bytes 524288 | tf_op jit(solution)/shard_map/all_to_all | solution.py:45
Sparse Core Ops, SparseCore 0:
  25.5 25.2 all-gather.1
  61.8 31.4 reduce-scatter.1
where the time goes:
time: 117 us
  waiting for transfers between devices  46.5 us (40%)
  blocking collectives  33.9 us (29%)
  matrix products  14.8 us (13%)
  between operations  13.5 us (12%)
  starting transfers between devices  4.65 us (4%)
  local copies, waits for them, and re-layouts  2.23 us (2%)
    all_gather x1, waiting for transfers between devices, per_device(): piece = lax.all_gather(arrived, 'tp', axis=1, tiled=True)  25.4 us
    all_gather x1, blocking collectives, per_device(): lax.all_gather(dense_hidden, 'tp', axis=1, tiled=True)  17.9 us
    all_to_all x1, blocking collectives, per_device(): lax.all_to_all(picked, 'ep', split_axis=0, concat_axis=1, tiled=True)  16 us
    reduce_scatter x1, waiting for transfers between devices, per_device(): lax.psum_scatter(lax.dot_general(w_down, hidden, (((0,), (1,)), ((), ()))...  11.8 us
    all_to_all x1, waiting for transfers between devices, per_device(): lax.all_to_all(summed, 'ep', split_axis=1, concat_axis=1, tiled=True)  9.33 us
    dot_general x1, matrix products, per_device(): lax.dot_general(w_down, hidden, (((0,), (1,)), ((), ())), preferred_eleme...  6.9 us
    all_to_all x1, starting transfers between devices, per_device(): lax.all_to_all(summed, 'ep', split_axis=1, concat_axis=1, tiled=True)  4.61 us
    dot_general x1, matrix products, per_device(): gate_val = jnp.dot(piece, w_gate, preferred_element_type=jnp.float32)  3.83 us
  transfers between devices with their start and end apart: 3, of which 3 were waited for; matrix products, arithmetic and copies ran while one was open for 2% of the time, Pallas kernels for 0%

commit v1 on v0

--- a/solution.py
+++ b/solution.py
@@ -1,10 +1,307 @@
+import functools
+
 import jax
 import jax.numpy as jnp
 from jax import lax
+from jax.experimental import pallas as pl
+from jax.experimental.pallas import tpu as pltpu
 from jax.sharding import PartitionSpec as P
 
-
-def per_device(
+BF = jnp.bfloat16
+F32 = jnp.float32
+
+
+def call(body, outs, limit_mib):
+    return pl.pallas_call(
+        body, out_shape=outs, compiler_params=pltpu.CompilerParams(vmem_limit_bytes=limit_mib << 20)
+    )
+
+
+def shape(dims, dtype):
+    return jax.ShapeDtypeStruct(dims, dtype)
+
+
+def dot(a, b):
+    return jnp.dot(a, b, preferred_element_type=F32)
+
+
+def hbm():
+    return pl.BlockSpec(memory_space=pltpu.HBM)
+
+
+def in_hbm(*arrays):
+    return [pltpu.with_memory_space_constraint(a, pltpu.HBM) for a in arrays]
+
+
+def vmem():
+    return pl.BlockSpec(memory_space=pltpu.VMEM)
+
+
+def table_row(table, ranks):
+    me = lax.axis_index("ep")
+    return jnp.concatenate([table[pl.ds(me ^ r, 1), :] for r in ranks], axis=1)
+
+
+def hits(table, ranks, rows):
+    slots = table_row(table, ranks)
+    return lax.broadcasted_iota(jnp.int32, (rows, slots.shape[1]), 0) == slots
+
+
+def select(hit, values):
+    sel = jnp.where(hit, 1.0, 0.0).astype(BF)
+    return lax.dot_general(
+        sel, values, (((0,), (0,)), ((), ())), preferred_element_type=F32
+    ).astype(BF)
+
+
+def pick_far_body(ranks, chosen, tokens, keep, give, table, cols, sems):
+    rows, width = cols.shape
+    at = pl.multiple_of(lax.axis_index("tp") * width, width)
+    one = pltpu.make_async_copy(chosen, table, sems.at[0])
+    two = pltpu.make_async_copy(tokens.at[:, pl.ds(at, width)], cols, sems.at[1])
+    one.start()
+    two.start()
+    one.wait()
+    hit = hits(table, ranks, rows)
+    two.wait()
+    got = select(hit, cols[...])
+    half = keep.shape[0]
+    keep[...] = got[:half]
+    give[...] = got[half:]
+
+
+def pick_near_body(near, order, chosen, weights, tokens, keep, give, comb, tok, table, table_w, tok_v, sems):
+    copies = (
+        pltpu.make_async_copy(chosen, table, sems.at[0]),
+        pltpu.make_async_copy(weights, table_w, sems.at[1]),
+        pltpu.make_async_copy(tokens, tok_v, sems.at[2]),
+    )
+    for c in copies:
+        c.start()
+    copies[0].wait()
+    copies[1].wait()
+    rows = tok_v.shape[0]
+    hit = hits(table, order, rows)
+    w = table_row(table_w, order)
+    high = w.astype(BF).astype(F32)
+    n = hit.shape[1]
+    comb[:, :n] = jnp.where(hit, high, 0.0).astype(BF)
+    comb[:, n:] = jnp.where(hit, w - high, 0.0).astype(BF)
+    sel = hits(table, near, rows)
+    copies[2].wait()
+    t = tok_v[...]
+    tok[...] = t
+    got = select(sel, t)
+    half = keep.shape[0]
+    keep[...] = got[:half]
+    give[...] = got[half:]
+
+
+def silu(v):
+    return v / (1.0 + jnp.exp(-v))
+
+
+def dense_in_body(tokens, w_in, w_gate, hidden, gate):
+    t = tokens[...]
+    hidden[...] = silu(dot(t, w_in[...])).astype(BF)
+    g = jnp.sum(t.astype(F32) * w_gate[...].astype(F32), axis=1, keepdims=True)
+    gate[...] = jax.nn.sigmoid(g)
+
+
+def down(hidden, w_down, outs):
+    tp = lax.axis_index("tp")
+    width = outs[0].shape[1]
+    for j in (3, 1, 2, 0):
+        cols = pl.ds(pl.multiple_of((tp ^ j) * width, width), width)
+        outs[j][...] = dot(hidden, w_down[:, cols]).astype(BF)
+
+
+def near_body(a, b, c, w_gate, w_up, w_down, v_gate, v_up, v_down, p0, p1, p2, p3, sems):
+    tiles = sems.shape[1]
+    copies = []
+    for i, (src, dst) in enumerate(((w_gate, v_gate), (w_up, v_up), (w_down, v_down))):
+        size = src.shape[0] // tiles
+        copies.append(
+            [
+                pltpu.make_async_copy(
+                    src.at[pl.ds(size * k, size), :], dst.at[pl.ds(size * k, size), :], sems.at[i, k]
+                )
+                for k in range(tiles)
+            ]
+        )
+    for k in range(tiles):
+        copies[0][k].start()
+        copies[1][k].start()
+    for k in range(tiles):
+        copies[2][k].start()
+    x = jnp.concatenate([a[...], b[...], c[...]], axis=0)
+    gate = up = 0.0
+    size = v_gate.shape[0] // tiles
+    for k in range(tiles):
+        v = x[:, size * k : size * (k + 1)]
+        copies[0][k].wait()
+        gate = gate + dot(v, v_gate[pl.ds(size * k, size), :])
+        copies[1][k].wait()
+        up = up + dot(v, v_up[pl.ds(size * k, size), :])
+    hidden = (silu(gate) * up).astype(BF)
+    for k in range(tiles):
+        copies[2][k].wait()
+    down(hidden, v_down, (p0, p1, p2, p3))
+
+
+def far_body(c0, c1, c2, c3, w_gate, w_up, w_down, p0, p1, p2, p3):
+    tp = lax.axis_index("tp")
+    width = c0.shape[1]
+    gate = up = 0.0
+    for j, chunk in enumerate((c0, c1, c2, c3)):
+        at = pl.ds(pl.multiple_of((tp ^ j) * width, width), width)
+        v = chunk[...]
+        gate = gate + dot(v, w_gate[at, :])
+        up = up + dot(v, w_up[at, :])
+    hidden = (silu(gate) * up).astype(BF)
+    down(hidden, w_down, (p0, p1, p2, p3))
+
+
+def dense_out_body(h0, h1, h2, h3, w_out, gate, val):
+    tp = lax.axis_index("tp")
+    width = h0.shape[1]
+    total = 0.0
+    for j, h in enumerate((h0, h1, h2, h3)):
+        rows = pl.ds(pl.multiple_of((tp ^ j) * width, width), width)
+        total = total + dot(h[...], w_out[rows, :])
+    val[...] = gate[...] * total
+
+
+def combine_body(own, other, comb, val, out):
+    half = own.shape[0]
+    n = 2 * half
+    a, b = own[...], other[...]
+    total = val[...]
+    for base in (0, n):
+        total = total + dot(comb[:, base : base + half], a)
+        total = total + dot(comb[:, base + half : base + n], b)
+    out[...] = total.astype(BF)
+
+
+def swap(v, axis, k):
+    return lax.ppermute(v, axis, [(i, i ^ k) for i in range(lax.axis_size(axis))])
+
+
+def fast(
+    tokens,
+    gate_proj,
+    up_proj,
+    down_proj,
+    side_input_weight,
+    dense_out,
+    dense_gate,
+    chosen_rows,
+    choice_weights,
+):
+    experts, slots = chosen_rows.shape
+    rows, model = tokens.shape
+    width = model // lax.axis_size("tp")
+    zs = experts // 2
+    w_gate, w_up, w_down = gate_proj[0], up_proj[0], down_proj[0]
+    order = tuple(range(0, experts, 2)) + tuple(range(1, experts, 2))
+    near = (0, 2, 1, 3)
+    far = tuple(range(4, experts, 2)) + tuple(range(5, experts, 2))
+    fk = zs - 2
+    dma = pltpu.SemaphoreType.DMA
+
+    keep_f, give_f = pl.pallas_call(
+        functools.partial(pick_far_body, far),
+        out_shape=(shape((fk * slots, width), BF),) * 2,
+        in_specs=[hbm(), hbm()],
+        out_specs=(vmem(), vmem()),
+        scratch_shapes=[
+            pltpu.VMEM((experts, slots), jnp.int32),
+            pltpu.VMEM((rows, width), BF),
+            dma((2,)),
+        ],
+        compiler_params=pltpu.CompilerParams(vmem_limit_bytes=8 << 20),
+        name="pick_far",
+    )(*in_hbm(chosen_rows, tokens))
+    got_f = swap(give_f, "ep", 1)
+    keep_n, give_n, comb, tok = pl.pallas_call(
+        functools.partial(pick_near_body, near, order),
+        out_shape=(
+            shape((2 * slots, model), BF),
+            shape((2 * slots, model), BF),
+            shape((rows, 2 * experts * slots), BF),
+            shape((rows, model), BF),
+        ),
+        in_specs=[hbm()] * 3,
+        out_specs=(vmem(),) * 4,
+        scratch_shapes=[
+            pltpu.VMEM((experts, slots), jnp.int32),
+            pltpu.VMEM((experts, slots), F32),
+            pltpu.VMEM((rows, model), BF),
+            dma((3,)),
+        ],
+        compiler_params=pltpu.CompilerParams(vmem_limit_bytes=12 << 20),
+        name="pick_near",
+    )(*in_hbm(chosen_rows, choice_weights, tokens))
+    got_n = swap(give_n, "ep", 1)
+
+    zf = []
+    for k in range(zs - 1, 1, -1):
+        at = (k - 2) * slots
+        block = jnp.concatenate([keep_f[at : at + slots], got_f[at : at + slots]], axis=0)
+        zf.append(swap(block, "ep", 2 * k))
+    z1 = swap(jnp.concatenate([keep_n[slots:], got_n[slots:]], axis=0), "ep", 2)
+
+    hidden_own, side_gate = call(
+        dense_in_body, (shape((rows, side_input_weight.shape[1]), BF), shape((rows, 1), F32)), 8
+    )(tok, side_input_weight, dense_gate.reshape(1, model))
+    hiddens = [hidden_own] + [swap(hidden_own, "tp", j) for j in (1, 2, 3)]
+
+    arrived = jnp.concatenate(zf, axis=0)
+    chunks = [arrived] + [swap(arrived, "tp", j) for j in (1, 2, 3)]
+
+    v_gate, v_up, v_down, *near_part = pl.pallas_call(
+        near_body,
+        out_shape=(
+            pltpu.VMEM(w_gate.shape, BF),
+            pltpu.VMEM(w_up.shape, BF),
+            pltpu.VMEM(w_down.shape, BF),
+        )
+        + (shape((4 * slots, width), BF),) * 4,
+        in_specs=[vmem()] * 3 + [hbm()] * 3,
+        out_specs=(vmem(),) * 7,
+        scratch_shapes=[dma((3, 4))],
+        compiler_params=pltpu.CompilerParams(vmem_limit_bytes=24 << 20),
+        name="near",
+    )(
+        keep_n[:slots],
+        got_n[:slots],
+        z1,
+        *in_hbm(w_gate, w_up, w_down),
+    )
+    far_part = call(far_body, (shape((2 * fk * slots, width), BF),) * 4, 24)(
+        *chunks, v_gate, v_up, v_down
+    )
+
+    def reduce(part):
+        sent = {j: swap(part[j], "tp", j) for j in (3, 1, 2)}
+        total = part[0].astype(F32) + sent[1].astype(F32)
+        return (total + sent[2].astype(F32) + sent[3].astype(F32)).astype(BF)
+
+    sum_f = reduce(far_part)
+    back = {}
+    for i, k in enumerate(range(zs - 1, 1, -1)):
+        back[k] = swap(sum_f[2 * slots * i : 2 * slots * (i + 1)], "ep", 2 * k)
+    sum_n = reduce(near_part)
+    back[0] = sum_n[: 2 * slots]
+    back[1] = swap(sum_n[2 * slots :], "ep", 2)
+    mine = jnp.concatenate([back[k][:slots] for k in range(zs)], axis=0)
+    theirs = swap(jnp.concatenate([back[k][slots:] for k in range(zs)], axis=0), "ep", 1)
+
+    val = call(dense_out_body, shape((rows, width), F32), 8)(*hiddens, dense_out, side_gate)
+    return call(combine_body, shape((rows, width), BF), 8)(mine, theirs, comb, val)
+
+
+def general(
     tokens,
     gate_proj,
     up_proj,
@@ -65,6 +362,23 @@
     return (routed + side_gate[:, None] * dense_val).astype(jnp.bfloat16)
 
 
+def per_device(tokens, gate_proj, *rest):
+    experts = lax.axis_size("ep")
+    fits = (
+        lax.axis_size("tp") == 4
+        and experts >= 4
+        and experts & (experts - 1) == 0
+        and tokens.shape[1] % (4 * 128) == 0
+        and gate_proj.shape[2] % 128 == 0
+        and rest[2].shape[1] % 128 == 0
+        and tokens.shape[0] <= 512
+        and rest[5].size <= 512
+    )
+    if not fits:
+        return general(tokens, gate_proj, *rest)
+    return fast(tokens, gate_proj, *rest)
+
+
 def solution(mesh):
     placed = (
         P("ep", None),

time: 117 us -> 59.5 us (0.51)
  blocking collectives: 33.9 us -> 0 us
  waiting for transfers between devices: 46.5 us -> 20.4 us
  starting transfers between devices: 4.65 us -> 26.1 us
  matrix products: 14.8 us -> 0 us
  between operations: 13.5 us -> 0.28 us
  Pallas kernels: 0 us -> 12.2 us
  local copies, waits for them, and re-layouts: 2.23 us -> 0.13 us
    ppermute x0 -> x21, starting transfers between devices: none -> 26.1 us  [swap(): lax.ppermute(v, axis, [(i, i ^ k) for i in range(lax.axis_size(axis))])]
    all_gather x1 -> x0, waiting for transfers between devices: 25.4 us -> none  [per_device(): piece = lax.all_gather(arrived, 'tp', axis=1, tiled=True)]
    ppermute x0 -> x21, waiting for transfers between devices: none -> 20.4 us  [swap(): lax.ppermute(v, axis, [(i, i ^ k) for i in range(lax.axis_size(axis))])]
    all_gather x1 -> x0, blocking collectives: 17.9 us -> none  [per_device(): lax.all_gather(dense_hidden, 'tp', axis=1, tiled=True)]
    all_to_all x1 -> x0, blocking collectives: 16 us -> none  [per_device(): lax.all_to_all(picked, 'ep', split_axis=0, concat_axis=1, tiled=True)]
    dot_general x7 -> x0, matrix products: 14.8 us -> none  [the longest x1 6.9 us: per_device(): lax.dot_general(w_down, hidden, (((0,), (1,)), ((), ())), preferred_eleme...]
    pallas_call x0 -> x7, Pallas kernels: none -> 12.2 us  [the longest x1 5.43 us: fast(): pl.pallas_call(near_body, out_shape=(pltpu.VMEM(w_gate.shape, BF), pltpu....]
    reduce_scatter x1 -> x0, waiting for transfers between devices: 11.8 us -> none  [per_device(): lax.psum_scatter(lax.dot_general(w_down, hidden, (((0,), (1,)), ((), ()))...]
  transfers between devices with their start and end apart: 3 -> 21, of which waited for: 3 -> 10; matrix products, arithmetic and copies ran while one was open for 2% -> 1% of each run, Pallas kernels for 0% -> 13%
where the time goes in v1:
time: 59.5 us; the launch traced here: 59.3 us
  starting transfers between devices  26.1 us (44%)
  waiting for transfers between devices  20.4 us (34%)
  Pallas kernels  12.2 us (21%)
    ppermute x21, starting transfers between devices, swap(): lax.ppermute(v, axis, [(i, i ^ k) for i in range(lax.axis_size(axis))])  26.1 us
    ppermute x21, waiting for transfers between devices, swap(): lax.ppermute(v, axis, [(i, i ^ k) for i in range(lax.axis_size(axis))])  20.4 us
    pallas_call x1, Pallas kernels, fast(): pl.pallas_call(near_body, out_shape=(pltpu.VMEM(w_gate.shape, BF), pltpu....  5.43 us
    pallas_call x1, Pallas kernels, fast(): call(far_body, (shape((2 * fk * slots, width), BF),) * 4, 24)  1.92 us
    pallas_call x1, Pallas kernels, fast(): pl.pallas_call(functools.partial(pick_near_body, near, order), out_shape=...  1.64 us
    pallas_call x1, Pallas kernels, fast(): pl.pallas_call(functools.partial(pick_far_body, far), out_shape=(shape((f...  1.19 us
  transfers between devices with their start and end apart: 21, of which 10 were waited for; matrix products, arithmetic and copies ran while one was open for 1% of the time, Pallas kernels for 13%

profile of v1, /device:TPU:0, one launch (start us, length us, event | category | flops | bytes accessed | tf_op | source)
XLA Modules:
  0.0 59.3 jit_solution(16552989741237430705)
XLA Ops:
  0.0 1.2 %pick_far.1 = (bf16[64,512]{1,0:T(8,128)(2,1)S(1)}, bf16[64,512]{1,0:T(8,128)(2,1)S(1)}) custom-call(s32[8,32]{1,0:T(8,128)} %chosen.3, bf16[256,2048]{1,0:T(8,128)(2,1)} %tokens.3), custom_call_target="tpu_custom_call" | custom-call | tf_op jit(solution)/shard_map/pick_far/pallas_call | solution.py:212
  1.2 0.6 collective-permute-start.6
  1.8 1.6 %pick_near.1 = (bf16[64,2048]{1,0:T(8,128)(2,1)S(1)}, bf16[64,2048]{1,0:T(8,128)(2,1)S(1)}, bf16[256,512]{1,0:T(8,128)(2,1)S(1)}, bf16[256,2048]{1,0:T(8,128)(2,1)S(1)}) custom-call(s32[8,32]{1,0:T(8,128)} %chosen.3, f32[8,32]{1,0:T(8,128)} %weights.1, bf16[256,2048]{1,0:T(8,128)(2,1)} %tokens.3), custom_call_target="tpu_custom_call" | custom-call | tf_op jit(solution)/shard_map/pick_near/pallas_call | solution.py:226
  3.4 0.1 collective-permute-start
  3.6 5.1 %collective-permute-start.7 = (bf16[64,512]{1,0:T(8,128)(2,1)S(1)}, bf16[64,512]{1,0:T(8,128)(2,1)S(1)}, u32[]{:S(2)}, u32[]{:S(2)}) collective-permute-start(bf16[64,512]{1,0:T(8,128)(2,1)S(1)} %pad_maximum_fusion.3), channel_id=1, source_target_pairs={{0,24},{4,28},{8,16},{12,20},{16,8},{20,12},{24,0},{28,4},{1,25},{... | collective-permute-start | bytes 196616 | tf_op jit(solution)/shard_map/ppermute | solution.py:187
  8.7 0.0 collective-permute-done
  8.8 0.7 %collective-permute-start.1 = (bf16[64,2048]{1,0:T(8,128)(2,1)S(1)}, bf16[64,2048]{1,0:T(8,128)(2,1)S(1)}, u32[]{:S(2)}, u32[]{:S(2)}) collective-permute-start(bf16[64,2048]{1,0:T(8,128)(2,1)S(1)} %pad_maximum_fusion), channel_id=1, source_target_pairs={{0,8},{4,12},{8,0},{12,4},{16,24},{20,28},{24,16},{28,20},{1,9},{5... | collective-permute-start | bytes 786440 | tf_op jit(solution)/shard_map/ppermute | solution.py:187
  9.5 1.8 %collective-permute-done.7 = bf16[64,512]{1,0:T(8,128)(2,1)S(1)} collective-permute-done((bf16[64,512]{1,0:T(8,128)(2,1)S(1)}, bf16[64,512]{1,0:T(8,128)(2,1)S(1)}, u32[]{:S(2)}, u32[]{:S(2)}) %collective-permute-start.7) | collective-permute-done | bytes 65568 | tf_op jit(solution)/shard_map/ppermute | solution.py:187
  11.2 3.3 %collective-permute-done.8 = bf16[64,512]{1,0:T(8,128)(2,1)S(1)} collective-permute-done((bf16[64,512]{1,0:T(8,128)(2,1)S(1)}, bf16[64,512]{1,0:T(8,128)(2,1)S(1)}, u32[]{:S(2)}, u32[]{:S(2)}) %collective-permute-start.8) | collective-permute-done | bytes 65568 | tf_op jit(solution)/shard_map/ppermute | solution.py:187
  14.6 2.4 %collective-permute-start.11 = (bf16[128,512]{1,0:T(8,128)(2,1)S(1)}, bf16[128,512]{1,0:T(8,128)(2,1)S(1)}, u32[]{:S(2)}, u32[]{:S(2)}) collective-permute-start(bf16[128,512]{1,0:T(8,128)(2,1)S(1)} %constant_dynamic-update-slice_fusion.c0), channel_id=1, source_target_pairs={{0,3},{1,2},{2,1},{3,0},{4,7},{5,6},{6,5},{7,4},{8,11},{9,10},{10,... | collective-permute-start | bytes 393224 | tf_op jit(solution)/shard_map/ppermute | solution.py:187
  17.1 0.5 collective-permute-start.10
  17.6 0.5 collective-permute-start.9
  18.1 0.1 collective-permute-done.1.c
  18.2 5.4 %near.1 = (bf16[2048,1024]{1,0:T(8,128)(2,1)S(1)}, bf16[2048,1024]{1,0:T(8,128)(2,1)S(1)}, bf16[1024,2048]{1,0:T(8,128)(2,1)S(1)}, bf16[128,512]{1,0:T(8,128)(2,...) custom-call(bf16[32,2048]{1,0:T(8,128)(2,1)S(1)} %get-tuple-element.44.a, ...), custom_call_target="tpu_custom_call" | custom-call | tf_op jit(solution)/shard_map/near/pallas_call | solution.py:262
  23.6 0.0 collective-permute-done.11.c3
  23.7 0.0 collective-permute-done.10.c2
  23.7 0.0 copy-start.2
  23.7 0.0 copy-start
  23.7 1.9 %shard_map.91 = (bf16[128,512]{1,0:T(8,128)(2,1)S(1)}, bf16[128,512]{1,0:T(8,128)(2,1)S(1)}, bf16[128,512]{1,0:T(8,128)(2,1)S(1)}, bf16[128,512]{1,0:T(8,128)(2,1)S(1)}) custom-call(bf16[128,512]{1,0:T(8,128)(2,1)S(1)} %constant_dynamic-update-slice_fusion.c0, bf16[128,512]{1,0:T(8,128)(2,1)S(1)} %collective-permute-done.9.c1, ...), custom_call_target="tpu_custom_call" | custom-call | tf_op jit(solution)/shard_map/pallas_call | solution.py:281
  25.6 0.0 copy-start.1
  25.6 1.6 %collective-permute-start.12 = (bf16[128,512]{1,0:T(8,128)(2,1)S(1)}, bf16[128,512]{1,0:T(8,128)(2,1)S(1)}, u32[]{:S(2)}, u32[]{:S(2)}) collective-permute-start(bf16[128,512]{1,0:T(8,128)(2,1)S(1)} %get-tuple-element.36), channel_id=1, source_target_pairs={{0,1},{1,0},{2,3},{3,2},{4,5},{5,4},{6,7},{7,6},{8,9},{9,8},{10,11... | collective-permute-start | bytes 393224 | tf_op jit(solution)/shard_map/ppermute | solution.py:187
  27.3 1.5 %collective-permute-start.13 = (bf16[128,512]{1,0:T(8,128)(2,1)S(1)}, bf16[128,512]{1,0:T(8,128)(2,1)S(1)}, u32[]{:S(2)}, u32[]{:S(2)}) collective-permute-start(bf16[128,512]{1,0:T(8,128)(2,1)S(1)} %get-tuple-element.37), channel_id=1, source_target_pairs={{0,2},{1,3},{2,0},{3,1},{4,6},{5,7},{6,4},{7,5},{8,10},{9,11},{10,... | collective-permute-start | bytes 393224 | tf_op jit(solution)/shard_map/ppermute | solution.py:187
  28.8 0.4 collective-permute-start.14
  29.2 0.5 shard_map.92
  29.7 2.6 %collective-permute-start.20 = (bf16[256,256]{1,0:T(8,128)(2,1)S(1)}, bf16[256,256]{1,0:T(8,128)(2,1)S(1)}, u32[]{:S(2)}, u32[]{:S(2)}) collective-permute-start(bf16[256,256]{1,0:T(8,128)(2,1)S(1)} %get-tuple-element.41.h0), channel_id=1, source_target_pairs={{0,3},{1,2},{2,1},{3,0},{4,7},{5,6},{6,5},{7,4},{8,11},{9,10},{10,... | collective-permute-start | bytes 393224 | tf_op jit(solution)/shard_map/ppermute | solution.py:187
  32.3 0.5 collective-permute-start.19
  32.8 0.0 collective-permute-done.12
  32.8 0.8 %collective-permute-start.2 = (bf16[128,512]{1,0:T(8,128)(2,1)S(1)}, bf16[128,512]{1,0:T(8,128)(2,1)S(1)}, u32[]{:S(2)}, u32[]{:S(2)}) collective-permute-start(bf16[128,512]{1,0:T(8,128)(2,1)S(1)} %get-tuple-element.27), channel_id=1, source_target_pairs={{0,1},{1,0},{2,3},{3,2},{4,5},{5,4},{6,7},{7,6},{8,9},{9,8},{10,11... | collective-permute-start | bytes 393224 | tf_op jit(solution)/shard_map/ppermute | solution.py:187
  33.6 4.5 %collective-permute-done.13 = bf16[128,512]{1,0:T(8,128)(2,1)S(1)} collective-permute-done((bf16[128,512]{1,0:T(8,128)(2,1)S(1)}, bf16[128,512]{1,0:T(8,128)(2,1)S(1)}, u32[]{:S(2)}, u32[]{:S(2)}) %collective-permute-start.13) | collective-permute-done | bytes 131104 | tf_op jit(solution)/shard_map/ppermute | solution.py:187
  38.2 3.0 %collective-permute-start.3 = (bf16[128,512]{1,0:T(8,128)(2,1)S(1)}, bf16[128,512]{1,0:T(8,128)(2,1)S(1)}, u32[]{:S(2)}, u32[]{:S(2)}) collective-permute-start(bf16[128,512]{1,0:T(8,128)(2,1)S(1)} %get-tuple-element.28), channel_id=1, source_target_pairs={{0,2},{1,3},{2,0},{3,1},{4,6},{5,7},{6,4},{7,5},{8,10},{9,11},{10,... | collective-permute-start | bytes 393224 | tf_op jit(solution)/shard_map/ppermute | solution.py:187
  41.1 0.0 collective-permute-done.14
  41.2 0.0 collective-permute-start.4
  41.2 0.1 add_convert_fusion
  41.3 1.5 %collective-permute-start.18 = (bf16[256,256]{1,0:T(8,128)(2,1)S(1)}, bf16[256,256]{1,0:T(8,128)(2,1)S(1)}, u32[]{:S(2)}, u32[]{:S(2)}) collective-permute-start(bf16[256,256]{1,0:T(8,128)(2,1)S(1)} %get-tuple-element.41.h0), channel_id=1, source_target_pairs={{0,1},{1,0},{2,3},{3,2},{4,5},{5,4},{6,7},{7,6},{8,9},{9,8},{10,11... | collective-permute-start | bytes 393224 | tf_op jit(solution)/shard_map/ppermute | solution.py:187
  42.8 2.3 %collective-permute-done.3 = bf16[128,512]{1,0:T(8,128)(2,1)S(1)} collective-permute-done((bf16[128,512]{1,0:T(8,128)(2,1)S(1)}, bf16[128,512]{1,0:T(8,128)(2,1)S(1)}, u32[]{:S(2)}, u32[]{:S(2)}) %collective-permute-start.3) | collective-permute-done | bytes 131104 | tf_op jit(solution)/shard_map/ppermute | solution.py:187
  45.1 1.0 %collective-permute-start.15 = (bf16[64,512]{1,0:T(8,128)(2,1)S(1)}, bf16[64,512]{1,0:T(8,128)(2,1)S(1)}, u32[]{:S(2)}, u32[]{:S(2)}) collective-permute-start(bf16[64,512]{1,0:T(8,128)(2,1)S(1)} %get-tuple-element.49), channel_id=1, source_target_pairs={{0,16},{4,20},{8,24},{12,28},{16,0},{20,4},{24,8},{28,12},{1,17},{... | collective-permute-start | bytes 196616 | tf_op jit(solution)/shard_map/ppermute | solution.py:187
  46.1 0.9 %collective-permute-done.4 = bf16[128,512]{1,0:T(8,128)(2,1)S(1)} collective-permute-done((bf16[128,512]{1,0:T(8,128)(2,1)S(1)}, bf16[128,512]{1,0:T(8,128)(2,1)S(1)}, u32[]{:S(2)}, u32[]{:S(2)}) %collective-permute-start.4) | collective-permute-done | bytes 131104 | tf_op jit(solution)/shard_map/ppermute | solution.py:187
  47.0 0.1 add_convert_fusion.1
  47.1 3.0 %collective-permute-start.16 = (bf16[64,512]{1,0:T(8,128)(2,1)S(1)}, bf16[64,512]{1,0:T(8,128)(2,1)S(1)}, u32[]{:S(2)}, u32[]{:S(2)}) collective-permute-start(bf16[64,512]{1,0:T(8,128)(2,1)S(1)} %get-tuple-element.50), channel_id=1, source_target_pairs={{0,24},{4,28},{8,16},{12,20},{16,8},{20,12},{24,0},{28,4},{1,25},{... | collective-permute-start | bytes 196616 | tf_op jit(solution)/shard_map/ppermute | solution.py:187
  50.1 2.4 %collective-permute-done.15 = bf16[64,512]{1,0:T(8,128)(2,1)S(1)} collective-permute-done((bf16[64,512]{1,0:T(8,128)(2,1)S(1)}, bf16[64,512]{1,0:T(8,128)(2,1)S(1)}, u32[]{:S(2)}, u32[]{:S(2)}) %collective-permute-start.15) | collective-permute-done | bytes 65568 | tf_op jit(solution)/shard_map/ppermute | solution.py:187
  52.5 0.0 collective-permute-start.5
  52.5 1.0 %collective-permute-done.16 = bf16[64,512]{1,0:T(8,128)(2,1)S(1)} collective-permute-done((bf16[64,512]{1,0:T(8,128)(2,1)S(1)}, bf16[64,512]{1,0:T(8,128)(2,1)S(1)}, u32[]{:S(2)}, u32[]{:S(2)}) %collective-permute-start.16) | collective-permute-done | bytes 65568 | tf_op jit(solution)/shard_map/ppermute | solution.py:187
  53.5 3.3 %collective-permute-done.5 = bf16[64,512]{1,0:T(8,128)(2,1)S(1)} collective-permute-done((bf16[64,512]{1,0:T(8,128)(2,1)S(1)}, bf16[64,512]{1,0:T(8,128)(2,1)S(1)}, u32[]{:S(2)}, u32[]{:S(2)}) %collective-permute-start.5) | collective-permute-done | bytes 65568 | tf_op jit(solution)/shard_map/ppermute | solution.py:187
  56.8 0.1 collective-permute-start.17
  56.9 0.0 collective-permute-done.20.h3
  56.9 0.4 shard_map.93.val
  57.4 0.8 %collective-permute-done.17.other = bf16[128,512]{1,0:T(8,128)(2,1)S(1)} collective-permute-done((bf16[128,512]{1,0:T(8,128)(2,1)S(1)}, bf16[128,512]{1,0:T(8,128)(2,1)S(1)}, u32[]{:S(2)}, u32[]{:S(2)}) %collective-permute-start.17) | collective-permute-done | bytes 131104 | tf_op jit(solution)/shard_map/ppermute | solution.py:187
  58.2 1.1 %shard_map.94 = bf16[256,512]{1,0:T(8,128)(2,1)} custom-call(bf16[128,512]{1,0:T(8,128)(2,1)S(1)} %pad_maximum_fusion.1.own, bf16[128,512]{1,0:T(8,128)(2,1)S(1)} %collective-permute-done.17.other, bf16[256,512]{1,0:T(8,128)(2,1)S(1)} %get-tuple-element.39.comb, f32[256,512]{1,0:T(8,128)S(1)} %shard_map.93.val), custom_call_target="tpu_custom_call" | custom-call | tf_op jit(solution)/shard_map/pallas_call | solution.py:301
  (27 shorter events, 0.2 us)
Async XLA Ops:
  1.2 2.3 %collective-permute-start.6 = (bf16[64,512]{1,0:T(8,128)(2,1)S(1)}, bf16[64,512]{1,0:T(8,128)(2,1)S(1)}, u32[]{:S(2)}, u32[]{:S(2)}) collective-permute-start(bf16[64,512]{1,0:T(8,128)(2,1)S(1)} %get-tuple-element.31), channel_id=1, source_target_pairs={{0,4},{4,0},{8,12},{12,8},{16,20},{20,16},{24,28},{28,24},{1,5},{5... | collective-permute-start | bytes 196616 | tf_op jit(solution)/shard_map/ppermute | solution.py:187
  3.4 5.3 %collective-permute-start = (bf16[64,2048]{1,0:T(8,128)(2,1)S(1)}, bf16[64,2048]{1,0:T(8,128)(2,1)S(1)}, u32[]{:S(2)}, u32[]{:S(2)}) collective-permute-start(bf16[64,2048]{1,0:T(8,128)(2,1)S(1)} %get-tuple-element.25), channel_id=1, source_target_pairs={{0,4},{4,0},{8,12},{12,8},{16,20},{20,16},{24,28},{28,24},{1,5},{5... | collective-permute-start | bytes 786440 | tf_op jit(solution)/shard_map/ppermute | solution.py:187
  3.6 7.7 %collective-permute-start.7 = (bf16[64,512]{1,0:T(8,128)(2,1)S(1)}, bf16[64,512]{1,0:T(8,128)(2,1)S(1)}, u32[]{:S(2)}, u32[]{:S(2)}) collective-permute-start(bf16[64,512]{1,0:T(8,128)(2,1)S(1)} %pad_maximum_fusion.3), channel_id=1, source_target_pairs={{0,24},{4,28},{8,16},{12,20},{16,8},{20,12},{24,0},{28,4},{1,25},{... | collective-permute-start | bytes 196616 | tf_op jit(solution)/shard_map/ppermute | solution.py:187
  8.7 5.9 %collective-permute-start.8 = (bf16[64,512]{1,0:T(8,128)(2,1)S(1)}, bf16[64,512]{1,0:T(8,128)(2,1)S(1)}, u32[]{:S(2)}, u32[]{:S(2)}) collective-permute-start(bf16[64,512]{1,0:T(8,128)(2,1)S(1)} %pad_maximum_fusion.4), channel_id=1, source_target_pairs={{0,16},{4,20},{8,24},{12,28},{16,0},{20,4},{24,8},{28,12},{1,17},{... | collective-permute-start | bytes 196616 | tf_op jit(solution)/shard_map/ppermute | solution.py:187
  8.8 9.4 %collective-permute-start.1 = (bf16[64,2048]{1,0:T(8,128)(2,1)S(1)}, bf16[64,2048]{1,0:T(8,128)(2,1)S(1)}, u32[]{:S(2)}, u32[]{:S(2)}) collective-permute-start(bf16[64,2048]{1,0:T(8,128)(2,1)S(1)} %pad_maximum_fusion), channel_id=1, source_target_pairs={{0,8},{4,12},{8,0},{12,4},{16,24},{20,28},{24,16},{28,20},{1,9},{5... | collective-permute-start | bytes 786440 | tf_op jit(solution)/shard_map/ppermute | solution.py:187
  14.6 9.0 %collective-permute-start.11 = (bf16[128,512]{1,0:T(8,128)(2,1)S(1)}, bf16[128,512]{1,0:T(8,128)(2,1)S(1)}, u32[]{:S(2)}, u32[]{:S(2)}) collective-permute-start(bf16[128,512]{1,0:T(8,128)(2,1)S(1)} %constant_dynamic-update-slice_fusion.c0), channel_id=1, source_target_pairs={{0,3},{1,2},{2,1},{3,0},{4,7},{5,6},{6,5},{7,4},{8,11},{9,10},{10,... | collective-permute-start | bytes 393224 | tf_op jit(solution)/shard_map/ppermute | solution.py:187
  17.1 6.6 %collective-permute-start.10 = (bf16[128,512]{1,0:T(8,128)(2,1)S(1)}, bf16[128,512]{1,0:T(8,128)(2,1)S(1)}, u32[]{:S(2)}, u32[]{:S(2)}) collective-permute-start(bf16[128,512]{1,0:T(8,128)(2,1)S(1)} %constant_dynamic-update-slice_fusion.c0), channel_id=1, source_target_pairs={{0,2},{1,3},{2,0},{3,1},{4,6},{5,7},{6,4},{7,5},{8,10},{9,11},{10,... | collective-permute-start | bytes 393224 | tf_op jit(solution)/shard_map/ppermute | solution.py:187
  17.6 6.1 %collective-permute-start.9 = (bf16[128,512]{1,0:T(8,128)(2,1)S(1)}, bf16[128,512]{1,0:T(8,128)(2,1)S(1)}, u32[]{:S(2)}, u32[]{:S(2)}) collective-permute-start(bf16[128,512]{1,0:T(8,128)(2,1)S(1)} %constant_dynamic-update-slice_fusion.c0), channel_id=1, source_target_pairs={{0,1},{1,0},{2,3},{3,2},{4,5},{5,4},{6,7},{7,6},{8,9},{9,8},{10,11... | collective-permute-start | bytes 393224 | tf_op jit(solution)/shard_map/ppermute | solution.py:187
  23.7 5.5 %copy-start.2 = (bf16[2048]{0:T(1024)(128)(2,1)S(1)}, bf16[2048]{0:T(1024)(128)(2,1)}, u32[]{:S(2)}) copy-start(bf16[2048]{0:T(1024)(128)(2,1)} %param.15) | copy-start | bytes 12292
  23.7 5.5 %copy-start = (bf16[2048,256]{1,0:T(8,128)(2,1)S(1)}, bf16[2048,256]{1,0:T(8,128)(2,1)}, u32[]{:S(2)}) copy-start(bf16[2048,256]{1,0:T(8,128)(2,1)} %w_in.1) | copy-start | bytes 3145732
  25.6 31.3 %copy-start.1 = (bf16[1024,512]{1,0:T(8,128)(2,1)S(1)}, bf16[1024,512]{1,0:T(8,128)(2,1)}, u32[]{:S(2)}) copy-start(bf16[1024,512]{1,0:T(8,128)(2,1)} %w_out.1) | copy-start | bytes 3145732
  25.6 7.2 %collective-permute-start.12 = (bf16[128,512]{1,0:T(8,128)(2,1)S(1)}, bf16[128,512]{1,0:T(8,128)(2,1)S(1)}, u32[]{:S(2)}, u32[]{:S(2)}) collective-permute-start(bf16[128,512]{1,0:T(8,128)(2,1)S(1)} %get-tuple-element.36), channel_id=1, source_target_pairs={{0,1},{1,0},{2,3},{3,2},{4,5},{5,4},{6,7},{7,6},{8,9},{9,8},{10,11... | collective-permute-start | bytes 393224 | tf_op jit(solution)/shard_map/ppermute | solution.py:187
  27.3 10.9 %collective-permute-start.13 = (bf16[128,512]{1,0:T(8,128)(2,1)S(1)}, bf16[128,512]{1,0:T(8,128)(2,1)S(1)}, u32[]{:S(2)}, u32[]{:S(2)}) collective-permute-start(bf16[128,512]{1,0:T(8,128)(2,1)S(1)} %get-tuple-element.37), channel_id=1, source_target_pairs={{0,2},{1,3},{2,0},{3,1},{4,6},{5,7},{6,4},{7,5},{8,10},{9,11},{10,... | collective-permute-start | bytes 393224 | tf_op jit(solution)/shard_map/ppermute | solution.py:187
  28.8 12.4 %collective-permute-start.14 = (bf16[128,512]{1,0:T(8,128)(2,1)S(1)}, bf16[128,512]{1,0:T(8,128)(2,1)S(1)}, u32[]{:S(2)}, u32[]{:S(2)}) collective-permute-start(bf16[128,512]{1,0:T(8,128)(2,1)S(1)} %get-tuple-element.38), channel_id=1, source_target_pairs={{0,3},{1,2},{2,1},{3,0},{4,7},{5,6},{6,5},{7,4},{8,11},{9,10},{10,... | collective-permute-start | bytes 393224 | tf_op jit(solution)/shard_map/ppermute | solution.py:187
  29.7 27.2 %collective-permute-start.20 = (bf16[256,256]{1,0:T(8,128)(2,1)S(1)}, bf16[256,256]{1,0:T(8,128)(2,1)S(1)}, u32[]{:S(2)}, u32[]{:S(2)}) collective-permute-start(bf16[256,256]{1,0:T(8,128)(2,1)S(1)} %get-tuple-element.41.h0), channel_id=1, source_target_pairs={{0,3},{1,2},{2,1},{3,0},{4,7},{5,6},{6,5},{7,4},{8,11},{9,10},{10,... | collective-permute-start | bytes 393224 | tf_op jit(solution)/shard_map/ppermute | solution.py:187
  32.3 24.6 %collective-permute-start.19 = (bf16[256,256]{1,0:T(8,128)(2,1)S(1)}, bf16[256,256]{1,0:T(8,128)(2,1)S(1)}, u32[]{:S(2)}, u32[]{:S(2)}) collective-permute-start(bf16[256,256]{1,0:T(8,128)(2,1)S(1)} %get-tuple-element.41.h0), channel_id=1, source_target_pairs={{0,2},{1,3},{2,0},{3,1},{4,6},{5,7},{6,4},{7,5},{8,10},{9,11},{10,... | collective-permute-start | bytes 393224 | tf_op jit(solution)/shard_map/ppermute | solution.py:187
  32.8 8.4 %collective-permute-start.2 = (bf16[128,512]{1,0:T(8,128)(2,1)S(1)}, bf16[128,512]{1,0:T(8,128)(2,1)S(1)}, u32[]{:S(2)}, u32[]{:S(2)}) collective-permute-start(bf16[128,512]{1,0:T(8,128)(2,1)S(1)} %get-tuple-element.27), channel_id=1, source_target_pairs={{0,1},{1,0},{2,3},{3,2},{4,5},{5,4},{6,7},{7,6},{8,9},{9,8},{10,11... | collective-permute-start | bytes 393224 | tf_op jit(solution)/shard_map/ppermute | solution.py:187
  38.2 6.9 %collective-permute-start.3 = (bf16[128,512]{1,0:T(8,128)(2,1)S(1)}, bf16[128,512]{1,0:T(8,128)(2,1)S(1)}, u32[]{:S(2)}, u32[]{:S(2)}) collective-permute-start(bf16[128,512]{1,0:T(8,128)(2,1)S(1)} %get-tuple-element.28), channel_id=1, source_target_pairs={{0,2},{1,3},{2,0},{3,1},{4,6},{5,7},{6,4},{7,5},{8,10},{9,11},{10,... | collective-permute-start | bytes 393224 | tf_op jit(solution)/shard_map/ppermute | solution.py:187
  41.2 5.9 %collective-permute-start.4 = (bf16[128,512]{1,0:T(8,128)(2,1)S(1)}, bf16[128,512]{1,0:T(8,128)(2,1)S(1)}, u32[]{:S(2)}, u32[]{:S(2)}) collective-permute-start(bf16[128,512]{1,0:T(8,128)(2,1)S(1)} %get-tuple-element.29), channel_id=1, source_target_pairs={{0,3},{1,2},{2,1},{3,0},{4,7},{5,6},{6,5},{7,4},{8,11},{9,10},{10,... | collective-permute-start | bytes 393224 | tf_op jit(solution)/shard_map/ppermute | solution.py:187
  41.3 15.6 %collective-permute-start.18 = (bf16[256,256]{1,0:T(8,128)(2,1)S(1)}, bf16[256,256]{1,0:T(8,128)(2,1)S(1)}, u32[]{:S(2)}, u32[]{:S(2)}) collective-permute-start(bf16[256,256]{1,0:T(8,128)(2,1)S(1)} %get-tuple-element.41.h0), channel_id=1, source_target_pairs={{0,1},{1,0},{2,3},{3,2},{4,5},{5,4},{6,7},{7,6},{8,9},{9,8},{10,11... | collective-permute-start | bytes 393224 | tf_op jit(solution)/shard_map/ppermute | solution.py:187
  45.1 7.4 %collective-permute-start.15 = (bf16[64,512]{1,0:T(8,128)(2,1)S(1)}, bf16[64,512]{1,0:T(8,128)(2,1)S(1)}, u32[]{:S(2)}, u32[]{:S(2)}) collective-permute-start(bf16[64,512]{1,0:T(8,128)(2,1)S(1)} %get-tuple-element.49), channel_id=1, source_target_pairs={{0,16},{4,20},{8,24},{12,28},{16,0},{20,4},{24,8},{28,12},{1,17},{... | collective-permute-start | bytes 196616 | tf_op jit(solution)/shard_map/ppermute | solution.py:187
  47.1 6.4 %collective-permute-start.16 = (bf16[64,512]{1,0:T(8,128)(2,1)S(1)}, bf16[64,512]{1,0:T(8,128)(2,1)S(1)}, u32[]{:S(2)}, u32[]{:S(2)}) collective-permute-start(bf16[64,512]{1,0:T(8,128)(2,1)S(1)} %get-tuple-element.50), channel_id=1, source_target_pairs={{0,24},{4,28},{8,16},{12,20},{16,8},{20,12},{24,0},{28,4},{1,25},{... | collective-permute-start | bytes 196616 | tf_op jit(solution)/shard_map/ppermute | solution.py:187
  52.5 4.3 %collective-permute-start.5 = (bf16[64,512]{1,0:T(8,128)(2,1)S(1)}, bf16[64,512]{1,0:T(8,128)(2,1)S(1)}, u32[]{:S(2)}, u32[]{:S(2)}) collective-permute-start(bf16[64,512]{1,0:T(8,128)(2,1)S(1)} %slice.82), channel_id=1, source_target_pairs={{0,8},{4,12},{8,0},{12,4},{16,24},{20,28},{24,16},{28,20},{1,9},{5... | collective-permute-start | bytes 196616 | tf_op jit(solution)/shard_map/ppermute | solution.py:187
  56.8 1.4 %collective-permute-start.17 = (bf16[128,512]{1,0:T(8,128)(2,1)S(1)}, bf16[128,512]{1,0:T(8,128)(2,1)S(1)}, u32[]{:S(2)}, u32[]{:S(2)}) collective-permute-start(bf16[128,512]{1,0:T(8,128)(2,1)S(1)} %pad_maximum_fusion.2), channel_id=1, source_target_pairs={{0,4},{4,0},{8,12},{12,8},{16,20},{20,16},{24,28},{28,24},{1,5},{5... | collective-permute-start | bytes 393224 | tf_op jit(solution)/shard_map/ppermute | solution.py:187

commit v2 on v0

--- a/solution.py
+++ b/solution.py
@@ -1,10 +1,281 @@
+import functools
+
 import jax
 import jax.numpy as jnp
 from jax import lax
+from jax.experimental import pallas as pl
+from jax.experimental.pallas import tpu as pltpu
 from jax.sharding import PartitionSpec as P
 
-
-def per_device(
+BF = jnp.bfloat16
+F32 = jnp.float32
+
+
+COST = pl.CostEstimate(flops=8_000_000_000, bytes_accessed=1 << 20, transcendentals=0)
+
+
+def call(body, outs, limit_mib, cost=None):
+    return pl.pallas_call(
+        body,
+        out_shape=outs,
+        cost_estimate=cost,
+        compiler_params=pltpu.CompilerParams(vmem_limit_bytes=limit_mib << 20),
+    )
+
+
+def shape(dims, dtype):
+    return jax.ShapeDtypeStruct(dims, dtype)
+
+
+def dot(a, b):
+    return jnp.dot(a, b, preferred_element_type=F32)
+
+
+def hbm():
+    return pl.BlockSpec(memory_space=pltpu.HBM)
+
+
+def in_hbm(*arrays):
+    return [pltpu.with_memory_space_constraint(a, pltpu.HBM) for a in arrays]
+
+
+def vmem():
+    return pl.BlockSpec(memory_space=pltpu.VMEM)
+
+
+def table_row(table, ranks):
+    me = lax.axis_index("ep")
+    return jnp.concatenate([table[pl.ds(me ^ r, 1), :] for r in ranks], axis=1)
+
+
+def hits(table, ranks, rows):
+    slots = table_row(table, ranks)
+    return lax.broadcasted_iota(jnp.int32, (rows, slots.shape[1]), 0) == slots
+
+
+def select(hit, values):
+    sel = jnp.where(hit, 1.0, 0.0).astype(BF)
+    return lax.dot_general(
+        sel, values, (((0,), (0,)), ((), ())), preferred_element_type=F32
+    ).astype(BF)
+
+
+def pick_far_body(ranks, chosen, tokens, keep, give, table, cols, sems):
+    rows = cols.shape[0]
+    width = cols.shape[1] // 2
+    copies = [pltpu.make_async_copy(chosen, table, sems.at[0])]
+    for i, j in enumerate((0, 3)):
+        copies.append(
+            pltpu.make_async_copy(
+                tokens.at[:, block(j, width)], cols.at[:, pl.ds(width * i, width)], sems.at[1 + i]
+            )
+        )
+    for c in copies:
+        c.start()
+    copies[0].wait()
+    hit = hits(table, ranks, rows)
+    for c in copies[1:]:
+        c.wait()
+    got = select(hit, cols[...])
+    half = keep.shape[0]
+    keep[...] = got[:half]
+    give[...] = got[half:]
+
+
+def pick_near_body(near, order, chosen, weights, tokens, keep, give, next_a, next_b, comb):
+    rows = tokens.shape[0]
+    got = select(hits(chosen, near, rows), tokens[...])
+    size = keep.shape[0]
+    for i, out in enumerate((keep, give, next_a, next_b)):
+        out[...] = got[size * i : size * (i + 1)]
+    hit = hits(chosen, order, rows)
+    w = table_row(weights, order)
+    high = w.astype(BF).astype(F32)
+    n = hit.shape[1]
+    comb[:, :n] = jnp.where(hit, high, 0.0).astype(BF)
+    comb[:, n:] = jnp.where(hit, w - high, 0.0).astype(BF)
+
+
+def silu(v):
+    return v / (1.0 + jnp.exp(-v))
+
+
+def dense_in_body(tokens, w_in, w_gate, hidden, gate):
+    t = tokens[...]
+    hidden[...] = silu(dot(t, w_in[...])).astype(BF)
+    w = w_gate[...].astype(F32)[None, :]
+    g = jnp.sum(t.astype(F32) * w, axis=1, keepdims=True)
+    gate[...] = jax.nn.sigmoid(g)
+
+
+def block(j, width):
+    return pl.ds(pl.multiple_of((lax.axis_index("tp") ^ j) * width, width), width)
+
+
+def down(hidden, w_down, outs):
+    for j, out in outs:
+        out[...] = dot(hidden, w_down[:, block(j, out.shape[1])]).astype(BF)
+
+
+def enter(chunks, w_gate, w_up):
+    gate = up = 0.0
+    for j, chunk in chunks:
+        v = chunk[...]
+        at = block(j, v.shape[1])
+        gate = gate + dot(v, w_gate[at, :])
+        up = up + dot(v, w_up[at, :])
+    return gate, up
+
+
+def near_body(a, b, c, d, w_gate, w_up, w_down, p0, p1, p2, p3):
+    x = jnp.concatenate([a[...], b[...], c[...], d[...]], axis=0)
+    gate, up = dot(x, w_gate[...]), dot(x, w_up[...])
+    down((silu(gate) * up).astype(BF), w_down, ((3, p3), (1, p1), (2, p2), (0, p0)))
+
+
+def far_a_body(c0, c1, w_gate, w_up, w_down, acc_gate, acc_up):
+    del w_down
+    acc_gate[...], acc_up[...] = enter(((0, c0), (1, c1)), w_gate, w_up)
+
+
+def far_b_body(c2, c3, acc_gate, acc_up, w_gate, w_up, w_down, hidden, p3):
+    gate, up = enter(((2, c2), (3, c3)), w_gate, w_up)
+    gate, up = gate + acc_gate[...], up + acc_up[...]
+    h = (silu(gate) * up).astype(BF)
+    hidden[...] = h
+    down(h, w_down, ((3, p3),))
+
+
+def far_c_body(hidden, w_down, p0, p1, p2):
+    down(hidden[...], w_down, ((1, p1), (2, p2), (0, p0)))
+
+
+def dense_out_body(h0, h1, h2, h3, w_out, gate, val):
+    total = 0.0
+    for j, h in enumerate((h0, h1, h2, h3)):
+        total = total + dot(h[...], w_out[block(j, h.shape[1]), :])
+    val[...] = gate[...] * total
+
+
+def combine_body(own, other, comb, val, out):
+    x = jnp.concatenate([own[...], other[...]], axis=0)
+    n = x.shape[0]
+    out[...] = (val[...] + dot(comb[:, :n], x) + dot(comb[:, n:], x)).astype(BF)
+
+
+def exchange(values):
+    got = {0: values[0]}
+    for j in (3, 1, 2):
+        if j < len(values):
+            got[j] = swap(values[j], "tp", j)
+    return [got[j] for j in range(len(values))]
+
+
+def swap(v, axis, k):
+    return lax.ppermute(v, axis, [(i, i ^ k) for i in range(lax.axis_size(axis))])
+
+
+def fast(
+    tokens,
+    gate_proj,
+    up_proj,
+    down_proj,
+    side_input_weight,
+    dense_out,
+    dense_gate,
+    chosen_rows,
+    choice_weights,
+):
+    experts, slots = chosen_rows.shape
+    rows, model = tokens.shape
+    width = model // lax.axis_size("tp")
+    zs = experts // 2
+    w_gate, w_up, w_down = gate_proj[0], up_proj[0], down_proj[0]
+    ff = w_gate.shape[1]
+    near = (0, 1, 2, 3)
+    order = tuple(range(0, experts, 2)) + tuple(range(1, experts, 2))
+    far = tuple(range(4, experts, 2)) + tuple(range(5, experts, 2))
+    fk = zs - 2
+    dma = pltpu.SemaphoreType.DMA
+
+    keep_f, give_f = pl.pallas_call(
+        functools.partial(pick_far_body, far),
+        out_shape=(shape((fk * slots, 2 * width), BF),) * 2,
+        in_specs=[hbm(), hbm()],
+        out_specs=(vmem(), vmem()),
+        scratch_shapes=[
+            pltpu.VMEM((experts, slots), jnp.int32),
+            pltpu.VMEM((rows, 2 * width), BF),
+            dma((3,)),
+        ],
+        compiler_params=pltpu.CompilerParams(vmem_limit_bytes=8 << 20),
+        cost_estimate=COST,
+        name="pick_far",
+    )(*in_hbm(chosen_rows, tokens))
+    got_f = swap(give_f, "ep", 1)
+    keep_n, give_n, next_a, next_b, comb = call(
+        functools.partial(pick_near_body, near, order),
+        (shape((slots, model), BF),) * 4
+        + (shape((rows, 2 * experts * slots), BF),),
+        8,
+        COST,
+    )(chosen_rows, choice_weights, tokens)
+    got_n = swap(give_n, "ep", 1)
+    z1a = swap(next_a, "ep", 2)
+    z1b = swap(next_b, "ep", 3)
+
+    waves = []
+    for cols in (slice(0, width), slice(width, 2 * width)):
+        got = []
+        for k in range(zs - 1, 1, -1):
+            at = (k - 2) * slots
+            rows_k = jnp.concatenate([keep_f[at : at + slots, cols], got_f[at : at + slots, cols]])
+            got.append(swap(rows_k, "ep", 2 * k))
+        waves.append(jnp.concatenate(got, axis=0))
+
+    hidden_own, side_gate = call(
+        dense_in_body,
+        (shape((rows, side_input_weight.shape[1]), BF), shape((rows, 1), F32)),
+        8,
+        COST,
+    )(tokens, side_input_weight, dense_gate)
+    hiddens = exchange([hidden_own] * 4)
+
+    chunks = exchange([waves[0]] * 3)
+
+    near_part = call(near_body, (shape((4 * slots, width), BF),) * 4, 8)(
+        keep_n, got_n, z1a, z1b, w_gate, w_up, w_down
+    )
+    far_rows = 2 * fk * slots
+    accs = call(far_a_body, (shape((far_rows, ff), F32),) * 2, 8)(
+        chunks[0], chunks[1], w_gate, w_up, w_down
+    )
+    hidden, part3 = call(
+        far_b_body, (shape((far_rows, ff), BF), shape((far_rows, width), BF)), 8
+    )(chunks[2], waves[1], *accs, w_gate, w_up, w_down)
+    far_part = call(far_c_body, (shape((far_rows, width), BF),) * 3, 8)(hidden, w_down)
+    far_part = [*far_part, part3]
+
+    def reduce(part):
+        sent = exchange(part)
+        total = part[0].astype(F32) + sent[1].astype(F32)
+        return (total + sent[2].astype(F32) + sent[3].astype(F32)).astype(BF)
+
+    sum_f = reduce(far_part)
+    back = {}
+    for i, k in enumerate(range(zs - 1, 1, -1)):
+        back[k] = swap(sum_f[2 * slots * i : 2 * slots * (i + 1)], "ep", 2 * k)
+    sum_n = reduce(near_part)
+    back[0] = sum_n[: 2 * slots]
+    back[1] = swap(sum_n[2 * slots :], "ep", 2)
+    mine = jnp.concatenate([back[k][:slots] for k in range(zs)], axis=0)
+    theirs = swap(jnp.concatenate([back[k][slots:] for k in range(zs)], axis=0), "ep", 1)
+
+    val = call(dense_out_body, shape((rows, width), F32), 8)(*hiddens, dense_out, side_gate)
+    return call(combine_body, shape((rows, width), BF), 8)(mine, theirs, comb, val)
+
+
+def general(
     tokens,
     gate_proj,
     up_proj,
@@ -65,6 +336,23 @@
     return (routed + side_gate[:, None] * dense_val).astype(jnp.bfloat16)
 
 
+def per_device(tokens, gate_proj, *rest):
+    experts = lax.axis_size("ep")
+    fits = (
+        lax.axis_size("tp") == 4
+        and experts >= 8
+        and experts & (experts - 1) == 0
+        and tokens.shape[1] % (4 * 128) == 0
+        and gate_proj.shape[2] % 128 == 0
+        and rest[2].shape[1] % 128 == 0
+        and tokens.shape[0] <= 512
+        and rest[5].size <= 512
+    )
+    if not fits:
+        return general(tokens, gate_proj, *rest)
+    return fast(tokens, gate_proj, *rest)
+
+
 def solution(mesh):
     placed = (
         P("ep", None),

time: 117 us -> 58.4 us (0.50)
  blocking collectives: 33.9 us -> 0 us
  waiting for transfers between devices: 46.5 us -> 17.5 us
  starting transfers between devices: 4.65 us -> 32.1 us
  matrix products: 14.8 us -> 0 us
  between operations: 13.5 us -> 0.28 us
  Pallas kernels: 0 us -> 8.1 us
  local copies, waits for them, and re-layouts: 2.23 us -> 0.11 us
    ppermute x0 -> x23, starting transfers between devices: none -> 32.1 us  [swap(): lax.ppermute(v, axis, [(i, i ^ k) for i in range(lax.axis_size(axis))])]
    all_gather x1 -> x0, waiting for transfers between devices: 25.4 us -> none  [per_device(): piece = lax.all_gather(arrived, 'tp', axis=1, tiled=True)]
    all_gather x1 -> x0, blocking collectives: 17.9 us -> none  [per_device(): lax.all_gather(dense_hidden, 'tp', axis=1, tiled=True)]
    ppermute x0 -> x23, waiting for transfers between devices: none -> 17.5 us  [swap(): lax.ppermute(v, axis, [(i, i ^ k) for i in range(lax.axis_size(axis))])]
    all_to_all x1 -> x0, blocking collectives: 16 us -> none  [per_device(): lax.all_to_all(picked, 'ep', split_axis=0, concat_axis=1, tiled=True)]
    dot_general x7 -> x0, matrix products: 14.8 us -> none  [the longest x1 6.9 us: per_device(): lax.dot_general(w_down, hidden, (((0,), (1,)), ((), ())), preferred_eleme...]
    reduce_scatter x1 -> x0, waiting for transfers between devices: 11.8 us -> none  [per_device(): lax.psum_scatter(lax.dot_general(w_down, hidden, (((0,), (1,)), ((), ()))...]
    all_to_all x1 -> x0, waiting for transfers between devices: 9.33 us -> none  [per_device(): lax.all_to_all(summed, 'ep', split_axis=1, concat_axis=1, tiled=True)]
  transfers between devices with their start and end apart: 3 -> 23, of which waited for: 3 -> 10; matrix products, arithmetic and copies ran while one was open for 2% -> 0% of each run, Pallas kernels for 0% -> 10%
where the time goes in v2:
time: 58.4 us; the launch traced here: 58.3 us
  starting transfers between devices  32.1 us (55%)
  waiting for transfers between devices  17.5 us (30%)
  Pallas kernels  8.1 us (14%)
    ppermute x23, starting transfers between devices, swap(): lax.ppermute(v, axis, [(i, i ^ k) for i in range(lax.axis_size(axis))])  32.1 us
    ppermute x23, waiting for transfers between devices, swap(): lax.ppermute(v, axis, [(i, i ^ k) for i in range(lax.axis_size(axis))])  17.5 us
    pallas_call x1, Pallas kernels, fast(): call(near_body, (shape((4 * slots, width), BF),) * 4, 8)  1.89 us
    pallas_call x1, Pallas kernels, fast(): pl.pallas_call(functools.partial(pick_far_body, far), out_shape=(shape((f...  1.42 us
  transfers between devices with their start and end apart: 23, of which 10 were waited for; matrix products, arithmetic and copies ran while one was open for 0% of the time, Pallas kernels for 10%

profile of v2, /device:TPU:0, one launch (start us, length us, event | category | flops | bytes accessed | tf_op | source)
XLA Modules:
  0.0 58.3 jit_solution(1113891905047678638)
XLA Ops:
  0.0 1.4 %pick_far.1 = (bf16[64,1024]{1,0:T(8,128)(2,1)S(1)}, bf16[64,1024]{1,0:T(8,128)(2,1)S(1)}) custom-call(s32[8,32]{1,0:T(8,128)} %chosen.3, bf16[256,2048]{1,0:T(8,128)(2,1)} %tokens.5), custom_call_target="tpu_custom_call" | custom-call | flops 8000000000 | bytes 1048576 | tf_op jit(solution)/shard_map/pick_far/pallas_call | solution.py:201
  1.4 0.0 copy-start.5
  1.4 0.0 copy-start.8
  1.5 0.6 collective-permute-start.7
  2.0 0.4 shard_map.91
  2.5 0.1 collective-permute-start
  2.6 3.0 %collective-permute-start.1 = (bf16[32,2048]{1,0:T(8,128)(2,1)S(1)}, bf16[32,2048]{1,0:T(8,128)(2,1)S(1)}, u32[]{:S(2)}, u32[]{:S(2)}) collective-permute-start(bf16[32,2048]{1,0:T(8,128)(2,1)S(1)} %get-tuple-element.27), channel_id=1, source_target_pairs={{0,8},{4,12},{8,0},{12,4},{16,24},{20,28},{24,16},{28,20},{1,9},{5... | collective-permute-start | bytes 393224 | tf_op jit(solution)/shard_map/ppermute | solution.py:175
  5.6 0.0 collective-permute-start.2
  5.6 0.5 shard_map.96
  6.2 0.0 collective-permute-done.7
  6.2 2.7 %collective-permute-start.9 = (bf16[64,512]{1,0:T(8,128)(2,1)S(1)}, bf16[64,512]{1,0:T(8,128)(2,1)S(1)}, u32[]{:S(2)}, u32[]{:S(2)}) collective-permute-start(bf16[64,512]{1,0:T(8,128)(2,1)S(1)} %pad_maximum_fusion.4), channel_id=1, source_target_pairs={{0,16},{4,20},{8,24},{12,28},{16,0},{20,4},{24,8},{28,12},{1,17},{... | collective-permute-start | bytes 196616 | tf_op jit(solution)/shard_map/ppermute | solution.py:175
  8.9 1.2 %collective-permute-start.8 = (bf16[64,512]{1,0:T(8,128)(2,1)S(1)}, bf16[64,512]{1,0:T(8,128)(2,1)S(1)}, u32[]{:S(2)}, u32[]{:S(2)}) collective-permute-start(bf16[64,512]{1,0:T(8,128)(2,1)S(1)} %pad_maximum_fusion.3), channel_id=1, source_target_pairs={{0,24},{4,28},{8,16},{12,20},{16,8},{20,12},{24,0},{28,4},{1,25},{... | collective-permute-start | bytes 196616 | tf_op jit(solution)/shard_map/ppermute | solution.py:175
  10.1 2.7 %collective-permute-start.11 = (bf16[64,512]{1,0:T(8,128)(2,1)S(1)}, bf16[64,512]{1,0:T(8,128)(2,1)S(1)}, u32[]{:S(2)}, u32[]{:S(2)}) collective-permute-start(bf16[64,512]{1,0:T(8,128)(2,1)S(1)} %pad_maximum_fusion.5), channel_id=1, source_target_pairs={{0,24},{4,28},{8,16},{12,20},{16,8},{20,12},{24,0},{28,4},{1,25},{... | collective-permute-start | bytes 196616 | tf_op jit(solution)/shard_map/ppermute | solution.py:175
  12.8 0.2 collective-permute-start.12
  13.0 1.9 %shard_map.92 = (bf16[128,512]{1,0:T(8,128)(2,1)S(1)}, bf16[128,512]{1,0:T(8,128)(2,1)S(1)}, bf16[128,512]{1,0:T(8,128)(2,1)S(1)}, bf16[128,512]{1,0:T(8,128)(2,1)S(1)}) custom-call(bf16[32,2048]{1,0:T(8,128)(2,1)S(1)} %get-tuple-element.25.a, bf16[32,2048]{1,0:T(8,128)(2,1)S(1)} %collective-permute-done.b, bf16[32,2048]{1,0:T(8,128)(2,1)S(1)} %collective-permute-done.1.c, ...), custom_call_target="tpu_custom_call" | custom-call | tf_op jit(solution)/shard_map/pallas_call | solution.py:246
  14.9 1.5 %collective-permute-start.3 = (bf16[128,512]{1,0:T(8,128)(2,1)S(1)}, bf16[128,512]{1,0:T(8,128)(2,1)S(1)}, u32[]{:S(2)}, u32[]{:S(2)}) collective-permute-start(bf16[128,512]{1,0:T(8,128)(2,1)S(1)} %get-tuple-element.30), channel_id=1, source_target_pairs={{0,1},{1,0},{2,3},{3,2},{4,5},{5,4},{6,7},{7,6},{8,9},{9,8},{10,11... | collective-permute-start | bytes 393224 | tf_op jit(solution)/shard_map/ppermute | solution.py:175
  16.4 1.7 %collective-permute-done.8 = bf16[64,512]{1,0:T(8,128)(2,1)S(1)} collective-permute-done((bf16[64,512]{1,0:T(8,128)(2,1)S(1)}, bf16[64,512]{1,0:T(8,128)(2,1)S(1)}, u32[]{:S(2)}, u32[]{:S(2)}) %collective-permute-start.8) | collective-permute-done | bytes 65568 | tf_op jit(solution)/shard_map/ppermute | solution.py:175
  18.1 1.5 %collective-permute-start.4 = (bf16[128,512]{1,0:T(8,128)(2,1)S(1)}, bf16[128,512]{1,0:T(8,128)(2,1)S(1)}, u32[]{:S(2)}, u32[]{:S(2)}) collective-permute-start(bf16[128,512]{1,0:T(8,128)(2,1)S(1)} %get-tuple-element.31), channel_id=1, source_target_pairs={{0,2},{1,3},{2,0},{3,1},{4,6},{5,7},{6,4},{7,5},{8,10},{9,11},{10,... | collective-permute-start | bytes 393224 | tf_op jit(solution)/shard_map/ppermute | solution.py:175
  19.7 1.5 %collective-permute-start.5 = (bf16[128,512]{1,0:T(8,128)(2,1)S(1)}, bf16[128,512]{1,0:T(8,128)(2,1)S(1)}, u32[]{:S(2)}, u32[]{:S(2)}) collective-permute-start(bf16[128,512]{1,0:T(8,128)(2,1)S(1)} %get-tuple-element.32), channel_id=1, source_target_pairs={{0,3},{1,2},{2,1},{3,0},{4,7},{5,6},{6,5},{7,4},{8,11},{9,10},{10,... | collective-permute-start | bytes 393224 | tf_op jit(solution)/shard_map/ppermute | solution.py:175
  21.2 0.6 %collective-permute-start.20 = (bf16[256,256]{1,0:T(8,128)(2,1)S(1)}, bf16[256,256]{1,0:T(8,128)(2,1)S(1)}, u32[]{:S(2)}, u32[]{:S(2)}) collective-permute-start(bf16[256,256]{1,0:T(8,128)(2,1)S(1)} %get-tuple-element.43.h0), channel_id=1, source_target_pairs={{0,1},{1,0},{2,3},{3,2},{4,5},{5,4},{6,7},{7,6},{8,9},{9,8},{10,11... | collective-permute-start | bytes 393224 | tf_op jit(solution)/shard_map/ppermute | solution.py:175
  21.8 0.8 %collective-permute-done.12 = bf16[64,512]{1,0:T(8,128)(2,1)S(1)} collective-permute-done((bf16[64,512]{1,0:T(8,128)(2,1)S(1)}, bf16[64,512]{1,0:T(8,128)(2,1)S(1)}, u32[]{:S(2)}, u32[]{:S(2)}) %collective-permute-start.12) | collective-permute-done | bytes 65568 | tf_op jit(solution)/shard_map/ppermute | solution.py:175
  22.6 1.5 %collective-permute-start.21 = (bf16[256,256]{1,0:T(8,128)(2,1)S(1)}, bf16[256,256]{1,0:T(8,128)(2,1)S(1)}, u32[]{:S(2)}, u32[]{:S(2)}) collective-permute-start(bf16[256,256]{1,0:T(8,128)(2,1)S(1)} %get-tuple-element.43.h0), channel_id=1, source_target_pairs={{0,2},{1,3},{2,0},{3,1},{4,6},{5,7},{6,4},{7,5},{8,10},{9,11},{10,... | collective-permute-start | bytes 393224 | tf_op jit(solution)/shard_map/ppermute | solution.py:175
  24.1 1.6 %collective-permute-start.13 = (bf16[128,512]{1,0:T(8,128)(2,1)S(1)}, bf16[128,512]{1,0:T(8,128)(2,1)S(1)}, u32[]{:S(2)}, u32[]{:S(2)}) collective-permute-start(bf16[128,512]{1,0:T(8,128)(2,1)S(1)} %constant_dynamic-update-slice_fusion.c0), channel_id=1, source_target_pairs={{0,1},{1,0},{2,3},{3,2},{4,5},{5,4},{6,7},{7,6},{8,9},{9,8},{10,11... | collective-permute-start | bytes 393224 | tf_op jit(solution)/shard_map/ppermute | solution.py:175
  25.7 0.5 collective-permute-start.10
  26.2 0.1 collective-permute-done.5
  26.2 0.1 add_convert_fusion.1
  26.3 2.9 %collective-permute-done.13.c1 = bf16[128,512]{1,0:T(8,128)(2,1)S(1)} collective-permute-done((bf16[128,512]{1,0:T(8,128)(2,1)S(1)}, bf16[128,512]{1,0:T(8,128)(2,1)S(1)}, u32[]{:S(2)}, u32[]{:S(2)}) %collective-permute-start.13) | collective-permute-done | bytes 131104 | tf_op jit(solution)/shard_map/ppermute | solution.py:175
  29.2 0.8 %shard_map.93 = (f32[128,1024]{1,0:T(8,128)S(1)}, f32[128,1024]{1,0:T(8,128)S(1)}) custom-call(bf16[128,512]{1,0:T(8,128)(2,1)S(1)} %constant_dynamic-update-slice_fusion.c0, bf16[128,512]{1,0:T(8,128)(2,1)S(1)} %collective-permute-done.13.c1, bf16[2048,1024]{1,0:T(8,128)(2,1)S(1)} %bitcast.8, bf16[2048,1024]{1,0:T(8,128)(2,1)S(1)} %bitcast.11, ...), custom_call_target="tpu_custom_call" | custom-call | tf_op jit(solution)/shard_map/pallas_call | solution.py:250
  30.0 1.5 %collective-permute-done.10.c2 = bf16[128,512]{1,0:T(8,128)(2,1)S(1)} collective-permute-done((bf16[128,512]{1,0:T(8,128)(2,1)S(1)}, bf16[128,512]{1,0:T(8,128)(2,1)S(1)}, u32[]{:S(2)}, u32[]{:S(2)}) %collective-permute-start.10) | collective-permute-done | bytes 131104 | tf_op jit(solution)/shard_map/ppermute | solution.py:175
  31.5 1.1 %shard_map.94 = (bf16[128,1024]{1,0:T(8,128)(2,1)S(1)}, bf16[128,512]{1,0:T(8,128)(2,1)S(1)}) custom-call(bf16[128,512]{1,0:T(8,128)(2,1)S(1)} %collective-permute-done.10.c2, bf16[128,512]{1,0:T(8,128)(2,1)S(1)} %pad_maximum_fusion.c3, f32[128,1024]{1,0:T(8,128)S(1)} %get-tuple-element.35.acc_gate, f32[128,1024]{1,0:T(8,128)S(1)} %get-tuple-element.36.acc_up, ...), custom_call_target="tpu_custom_call" | custom-call | tf_op jit(solution)/shard_map/pallas_call | solution.py:253
  32.6 0.0 copy-start.3
  32.6 0.6 %shard_map.95 = (bf16[128,512]{1,0:T(8,128)(2,1)S(1)}, bf16[128,512]{1,0:T(8,128)(2,1)S(1)}, bf16[128,512]{1,0:T(8,128)(2,1)S(1)}) custom-call(bf16[128,1024]{1,0:T(8,128)(2,1)S(1)} %get-tuple-element.37.hidden, bf16[1024,2048]{1,0:T(8,128)(2,1)S(1)} %bitcast.6), custom_call_target="tpu_custom_call" | custom-call | tf_op jit(solution)/shard_map/pallas_call | solution.py:256
  33.2 1.5 %collective-permute-start.14 = (bf16[128,512]{1,0:T(8,128)(2,1)S(1)}, bf16[128,512]{1,0:T(8,128)(2,1)S(1)}, u32[]{:S(2)}, u32[]{:S(2)}) collective-permute-start(bf16[128,512]{1,0:T(8,128)(2,1)S(1)} %get-tuple-element.39), channel_id=1, source_target_pairs={{0,1},{1,0},{2,3},{3,2},{4,5},{5,4},{6,7},{7,6},{8,9},{9,8},{10,11... | collective-permute-start | bytes 393224 | tf_op jit(solution)/shard_map/ppermute | solution.py:175
  34.7 0.7 %collective-permute-start.15 = (bf16[128,512]{1,0:T(8,128)(2,1)S(1)}, bf16[128,512]{1,0:T(8,128)(2,1)S(1)}, u32[]{:S(2)}, u32[]{:S(2)}) collective-permute-start(bf16[128,512]{1,0:T(8,128)(2,1)S(1)} %get-tuple-element.40), channel_id=1, source_target_pairs={{0,2},{1,3},{2,0},{3,1},{4,6},{5,7},{6,4},{7,5},{8,10},{9,11},{10,... | collective-permute-start | bytes 393224 | tf_op jit(solution)/shard_map/ppermute | solution.py:175
  35.4 1.3 %collective-permute-start.16 = (bf16[128,512]{1,0:T(8,128)(2,1)S(1)}, bf16[128,512]{1,0:T(8,128)(2,1)S(1)}, u32[]{:S(2)}, u32[]{:S(2)}) collective-permute-start(bf16[128,512]{1,0:T(8,128)(2,1)S(1)} %get-tuple-element.41), channel_id=1, source_target_pairs={{0,3},{1,2},{2,1},{3,0},{4,7},{5,6},{6,5},{7,4},{8,11},{9,10},{10,... | collective-permute-start | bytes 393224 | tf_op jit(solution)/shard_map/ppermute | solution.py:175
  36.7 1.8 %collective-permute-done.14 = bf16[128,512]{1,0:T(8,128)(2,1)S(1)} collective-permute-done((bf16[128,512]{1,0:T(8,128)(2,1)S(1)}, bf16[128,512]{1,0:T(8,128)(2,1)S(1)}, u32[]{:S(2)}, u32[]{:S(2)}) %collective-permute-start.14) | collective-permute-done | bytes 131104 | tf_op jit(solution)/shard_map/ppermute | solution.py:175
  38.6 2.5 %collective-permute-start.22 = (bf16[256,256]{1,0:T(8,128)(2,1)S(1)}, bf16[256,256]{1,0:T(8,128)(2,1)S(1)}, u32[]{:S(2)}, u32[]{:S(2)}) collective-permute-start(bf16[256,256]{1,0:T(8,128)(2,1)S(1)} %get-tuple-element.43.h0), channel_id=1, source_target_pairs={{0,3},{1,2},{2,1},{3,0},{4,7},{5,6},{6,5},{7,4},{8,11},{9,10},{10,... | collective-permute-start | bytes 393224 | tf_op jit(solution)/shard_map/ppermute | solution.py:175
  41.1 4.2 %collective-permute-done.15 = bf16[128,512]{1,0:T(8,128)(2,1)S(1)} collective-permute-done((bf16[128,512]{1,0:T(8,128)(2,1)S(1)}, bf16[128,512]{1,0:T(8,128)(2,1)S(1)}, u32[]{:S(2)}, u32[]{:S(2)}) %collective-permute-start.15) | collective-permute-done | bytes 131104 | tf_op jit(solution)/shard_map/ppermute | solution.py:175
  45.2 0.5 collective-permute-start.6
  45.7 0.1 add_convert_fusion
  45.8 2.7 %collective-permute-start.17 = (bf16[64,512]{1,0:T(8,128)(2,1)S(1)}, bf16[64,512]{1,0:T(8,128)(2,1)S(1)}, u32[]{:S(2)}, u32[]{:S(2)}) collective-permute-start(bf16[64,512]{1,0:T(8,128)(2,1)S(1)} %get-tuple-element.47), channel_id=1, source_target_pairs={{0,16},{4,20},{8,24},{12,28},{16,0},{20,4},{24,8},{28,12},{1,17},{... | collective-permute-start | bytes 196616 | tf_op jit(solution)/shard_map/ppermute | solution.py:175
  48.5 1.3 %collective-permute-done.6 = bf16[64,512]{1,0:T(8,128)(2,1)S(1)} collective-permute-done((bf16[64,512]{1,0:T(8,128)(2,1)S(1)}, bf16[64,512]{1,0:T(8,128)(2,1)S(1)}, u32[]{:S(2)}, u32[]{:S(2)}) %collective-permute-start.6) | collective-permute-done | bytes 65568 | tf_op jit(solution)/shard_map/ppermute | solution.py:175
  49.8 3.7 %collective-permute-start.18 = (bf16[64,512]{1,0:T(8,128)(2,1)S(1)}, bf16[64,512]{1,0:T(8,128)(2,1)S(1)}, u32[]{:S(2)}, u32[]{:S(2)}) collective-permute-start(bf16[64,512]{1,0:T(8,128)(2,1)S(1)} %get-tuple-element.48), channel_id=1, source_target_pairs={{0,24},{4,28},{8,16},{12,20},{16,8},{20,12},{24,0},{28,4},{1,25},{... | collective-permute-start | bytes 196616 | tf_op jit(solution)/shard_map/ppermute | solution.py:175
  53.4 2.4 %collective-permute-done.18 = bf16[64,512]{1,0:T(8,128)(2,1)S(1)} collective-permute-done((bf16[64,512]{1,0:T(8,128)(2,1)S(1)}, bf16[64,512]{1,0:T(8,128)(2,1)S(1)}, u32[]{:S(2)}, u32[]{:S(2)}) %collective-permute-start.18) | collective-permute-done | bytes 65568 | tf_op jit(solution)/shard_map/ppermute | solution.py:175
  55.8 0.1 collective-permute-start.19
  56.0 0.4 shard_map.97.val
  56.4 0.8 %collective-permute-done.19.other = bf16[128,512]{1,0:T(8,128)(2,1)S(1)} collective-permute-done((bf16[128,512]{1,0:T(8,128)(2,1)S(1)}, bf16[128,512]{1,0:T(8,128)(2,1)S(1)}, u32[]{:S(2)}, u32[]{:S(2)}) %collective-permute-start.19) | collective-permute-done | bytes 131104 | tf_op jit(solution)/shard_map/ppermute | solution.py:175
  57.3 1.0 %shard_map.98 = bf16[256,512]{1,0:T(8,128)(2,1)} custom-call(bf16[128,512]{1,0:T(8,128)(2,1)S(1)} %pad_maximum_fusion.1.own, bf16[128,512]{1,0:T(8,128)(2,1)S(1)} %collective-permute-done.19.other, bf16[256,512]{1,0:T(8,128)(2,1)S(1)} %get-tuple-element.42.comb, f32[256,512]{1,0:T(8,128)S(1)} %shard_map.97.val), custom_call_target="tpu_custom_call" | custom-call | tf_op jit(solution)/shard_map/pallas_call | solution.py:275
  (44 shorter events, 0.2 us)
Async XLA Ops:
  0.0 2.0 %copy-start.6 = (s32[8,32]{1,0:T(8,128)S(1)}, s32[8,32]{1,0:T(8,128)}, u32[]{:S(2)}) copy-start(s32[8,32]{1,0:T(8,128)} %chosen.3) | copy-start | bytes 3076
  0.0 2.0 %copy-start.4 = (bf16[256,2048]{1,0:T(8,128)(2,1)S(1)}, bf16[256,2048]{1,0:T(8,128)(2,1)}, u32[]{:S(2)}) copy-start(bf16[256,2048]{1,0:T(8,128)(2,1)} %tokens.5) | copy-start | bytes 3145732
  0.0 2.0 %copy-start.7 = (f32[8,32]{1,0:T(8,128)S(1)}, f32[8,32]{1,0:T(8,128)}, u32[]{:S(2)}) copy-start(f32[8,32]{1,0:T(8,128)} %weights.1) | copy-start | bytes 3076
  1.4 4.2 %copy-start.5 = (bf16[2048,256]{1,0:T(8,128)(2,1)S(1)}, bf16[2048,256]{1,0:T(8,128)(2,1)}, u32[]{:S(2)}) copy-start(bf16[2048,256]{1,0:T(8,128)(2,1)} %w_in.1) | copy-start | bytes 3145732
  1.4 4.2 %copy-start.8 = (bf16[2048]{0:T(1024)(128)(2,1)S(1)}, bf16[2048]{0:T(1024)(128)(2,1)}, u32[]{:S(2)}) copy-start(bf16[2048]{0:T(1024)(128)(2,1)} %w_gate.1) | copy-start | bytes 12292
  1.5 4.7 %collective-permute-start.7 = (bf16[64,1024]{1,0:T(8,128)(2,1)S(1)}, bf16[64,1024]{1,0:T(8,128)(2,1)S(1)}, u32[]{:S(2)}, u32[]{:S(2)}) collective-permute-start(bf16[64,1024]{1,0:T(8,128)(2,1)S(1)} %get-tuple-element.34), channel_id=1, source_target_pairs={{0,4},{4,0},{8,12},{12,8},{16,20},{20,16},{24,28},{28,24},{1,5},{5... | collective-permute-start | bytes 393224 | tf_op jit(solution)/shard_map/ppermute | solution.py:175
  2.5 7.6 %collective-permute-start = (bf16[32,2048]{1,0:T(8,128)(2,1)S(1)}, bf16[32,2048]{1,0:T(8,128)(2,1)S(1)}, u32[]{:S(2)}, u32[]{:S(2)}) collective-permute-start(bf16[32,2048]{1,0:T(8,128)(2,1)S(1)} %get-tuple-element.26), channel_id=1, source_target_pairs={{0,4},{4,0},{8,12},{12,8},{16,20},{20,16},{24,28},{28,24},{1,5},{5... | collective-permute-start | bytes 393224 | tf_op jit(solution)/shard_map/ppermute | solution.py:175
  2.6 10.2 %collective-permute-start.1 = (bf16[32,2048]{1,0:T(8,128)(2,1)S(1)}, bf16[32,2048]{1,0:T(8,128)(2,1)S(1)}, u32[]{:S(2)}, u32[]{:S(2)}) collective-permute-start(bf16[32,2048]{1,0:T(8,128)(2,1)S(1)} %get-tuple-element.27), channel_id=1, source_target_pairs={{0,8},{4,12},{8,0},{12,4},{16,24},{20,28},{24,16},{28,20},{1,9},{5... | collective-permute-start | bytes 393224 | tf_op jit(solution)/shard_map/ppermute | solution.py:175
  5.6 7.4 %copy-start = (bf16[1,1024,2048]{2,1,0:T(8,128)(2,1)S(1)}, bf16[1,1024,2048]{2,1,0:T(8,128)(2,1)}, u32[]{:S(2)}) copy-start(bf16[1,1024,2048]{2,1,0:T(8,128)(2,1)} %param.12) | copy-start | bytes 12582916
  5.6 7.4 %copy-start.1 = (bf16[1,2048,1024]{2,1,0:T(8,128)(2,1)S(1)}, bf16[1,2048,1024]{2,1,0:T(8,128)(2,1)}, u32[]{:S(2)}) copy-start(bf16[1,2048,1024]{2,1,0:T(8,128)(2,1)} %param.10) | copy-start | bytes 12582916
  5.6 7.4 %copy-start.2 = (bf16[1,2048,1024]{2,1,0:T(8,128)(2,1)S(1)}, bf16[1,2048,1024]{2,1,0:T(8,128)(2,1)}, u32[]{:S(2)}) copy-start(bf16[1,2048,1024]{2,1,0:T(8,128)(2,1)} %param.11) | copy-start | bytes 12582916
  5.6 7.4 %collective-permute-start.2 = (bf16[32,2048]{1,0:T(8,128)(2,1)S(1)}, bf16[32,2048]{1,0:T(8,128)(2,1)S(1)}, u32[]{:S(2)}, u32[]{:S(2)}) collective-permute-start(bf16[32,2048]{1,0:T(8,128)(2,1)S(1)} %get-tuple-element.28), channel_id=1, source_target_pairs={{0,12},{4,8},{8,4},{12,0},{16,28},{20,24},{24,20},{28,16},{1,13},{... | collective-permute-start | bytes 393224 | tf_op jit(solution)/shard_map/ppermute | solution.py:175
  6.2 13.4 %collective-permute-start.9 = (bf16[64,512]{1,0:T(8,128)(2,1)S(1)}, bf16[64,512]{1,0:T(8,128)(2,1)S(1)}, u32[]{:S(2)}, u32[]{:S(2)}) collective-permute-start(bf16[64,512]{1,0:T(8,128)(2,1)S(1)} %pad_maximum_fusion.4), channel_id=1, source_target_pairs={{0,16},{4,20},{8,24},{12,28},{16,0},{20,4},{24,8},{28,12},{1,17},{... | collective-permute-start | bytes 196616 | tf_op jit(solution)/shard_map/ppermute | solution.py:175
  8.9 9.3 %collective-permute-start.8 = (bf16[64,512]{1,0:T(8,128)(2,1)S(1)}, bf16[64,512]{1,0:T(8,128)(2,1)S(1)}, u32[]{:S(2)}, u32[]{:S(2)}) collective-permute-start(bf16[64,512]{1,0:T(8,128)(2,1)S(1)} %pad_maximum_fusion.3), channel_id=1, source_target_pairs={{0,24},{4,28},{8,16},{12,20},{16,8},{20,12},{24,0},{28,4},{1,25},{... | collective-permute-start | bytes 196616 | tf_op jit(solution)/shard_map/ppermute | solution.py:175
  10.1 11.1 %collective-permute-start.11 = (bf16[64,512]{1,0:T(8,128)(2,1)S(1)}, bf16[64,512]{1,0:T(8,128)(2,1)S(1)}, u32[]{:S(2)}, u32[]{:S(2)}) collective-permute-start(bf16[64,512]{1,0:T(8,128)(2,1)S(1)} %pad_maximum_fusion.5), channel_id=1, source_target_pairs={{0,24},{4,28},{8,16},{12,20},{16,8},{20,12},{24,0},{28,4},{1,25},{... | collective-permute-start | bytes 196616 | tf_op jit(solution)/shard_map/ppermute | solution.py:175
  12.8 9.8 %collective-permute-start.12 = (bf16[64,512]{1,0:T(8,128)(2,1)S(1)}, bf16[64,512]{1,0:T(8,128)(2,1)S(1)}, u32[]{:S(2)}, u32[]{:S(2)}) collective-permute-start(bf16[64,512]{1,0:T(8,128)(2,1)S(1)} %pad_maximum_fusion.6), channel_id=1, source_target_pairs={{0,16},{4,20},{8,24},{12,28},{16,0},{20,4},{24,8},{28,12},{1,17},{... | collective-permute-start | bytes 196616 | tf_op jit(solution)/shard_map/ppermute | solution.py:175
  14.9 9.2 %collective-permute-start.3 = (bf16[128,512]{1,0:T(8,128)(2,1)S(1)}, bf16[128,512]{1,0:T(8,128)(2,1)S(1)}, u32[]{:S(2)}, u32[]{:S(2)}) collective-permute-start(bf16[128,512]{1,0:T(8,128)(2,1)S(1)} %get-tuple-element.30), channel_id=1, source_target_pairs={{0,1},{1,0},{2,3},{3,2},{4,5},{5,4},{6,7},{7,6},{8,9},{9,8},{10,11... | collective-permute-start | bytes 393224 | tf_op jit(solution)/shard_map/ppermute | solution.py:175
  18.1 7.5 %collective-permute-start.4 = (bf16[128,512]{1,0:T(8,128)(2,1)S(1)}, bf16[128,512]{1,0:T(8,128)(2,1)S(1)}, u32[]{:S(2)}, u32[]{:S(2)}) collective-permute-start(bf16[128,512]{1,0:T(8,128)(2,1)S(1)} %get-tuple-element.31), channel_id=1, source_target_pairs={{0,2},{1,3},{2,0},{3,1},{4,6},{5,7},{6,4},{7,5},{8,10},{9,11},{10,... | collective-permute-start | bytes 393224 | tf_op jit(solution)/shard_map/ppermute | solution.py:175
  19.7 6.6 %collective-permute-start.5 = (bf16[128,512]{1,0:T(8,128)(2,1)S(1)}, bf16[128,512]{1,0:T(8,128)(2,1)S(1)}, u32[]{:S(2)}, u32[]{:S(2)}) collective-permute-start(bf16[128,512]{1,0:T(8,128)(2,1)S(1)} %get-tuple-element.32), channel_id=1, source_target_pairs={{0,3},{1,2},{2,1},{3,0},{4,7},{5,6},{6,5},{7,4},{8,11},{9,10},{10,... | collective-permute-start | bytes 393224 | tf_op jit(solution)/shard_map/ppermute | solution.py:175
  21.2 34.7 %collective-permute-start.20 = (bf16[256,256]{1,0:T(8,128)(2,1)S(1)}, bf16[256,256]{1,0:T(8,128)(2,1)S(1)}, u32[]{:S(2)}, u32[]{:S(2)}) collective-permute-start(bf16[256,256]{1,0:T(8,128)(2,1)S(1)} %get-tuple-element.43.h0), channel_id=1, source_target_pairs={{0,1},{1,0},{2,3},{3,2},{4,5},{5,4},{6,7},{7,6},{8,9},{9,8},{10,11... | collective-permute-start | bytes 393224 | tf_op jit(solution)/shard_map/ppermute | solution.py:175
  22.6 33.4 %collective-permute-start.21 = (bf16[256,256]{1,0:T(8,128)(2,1)S(1)}, bf16[256,256]{1,0:T(8,128)(2,1)S(1)}, u32[]{:S(2)}, u32[]{:S(2)}) collective-permute-start(bf16[256,256]{1,0:T(8,128)(2,1)S(1)} %get-tuple-element.43.h0), channel_id=1, source_target_pairs={{0,2},{1,3},{2,0},{3,1},{4,6},{5,7},{6,4},{7,5},{8,10},{9,11},{10,... | collective-permute-start | bytes 393224 | tf_op jit(solution)/shard_map/ppermute | solution.py:175
  24.1 5.1 %collective-permute-start.13 = (bf16[128,512]{1,0:T(8,128)(2,1)S(1)}, bf16[128,512]{1,0:T(8,128)(2,1)S(1)}, u32[]{:S(2)}, u32[]{:S(2)}) collective-permute-start(bf16[128,512]{1,0:T(8,128)(2,1)S(1)} %constant_dynamic-update-slice_fusion.c0), channel_id=1, source_target_pairs={{0,1},{1,0},{2,3},{3,2},{4,5},{5,4},{6,7},{7,6},{8,9},{9,8},{10,11... | collective-permute-start | bytes 393224 | tf_op jit(solution)/shard_map/ppermute | solution.py:175
  25.7 5.8 %collective-permute-start.10 = (bf16[128,512]{1,0:T(8,128)(2,1)S(1)}, bf16[128,512]{1,0:T(8,128)(2,1)S(1)}, u32[]{:S(2)}, u32[]{:S(2)}) collective-permute-start(bf16[128,512]{1,0:T(8,128)(2,1)S(1)} %constant_dynamic-update-slice_fusion.c0), channel_id=1, source_target_pairs={{0,2},{1,3},{2,0},{3,1},{4,6},{5,7},{6,4},{7,5},{8,10},{9,11},{10,... | collective-permute-start | bytes 393224 | tf_op jit(solution)/shard_map/ppermute | solution.py:175
  32.6 23.4 %copy-start.3 = (bf16[1024,512]{1,0:T(8,128)(2,1)S(1)}, bf16[1024,512]{1,0:T(8,128)(2,1)}, u32[]{:S(2)}) copy-start(bf16[1024,512]{1,0:T(8,128)(2,1)} %w_out.1) | copy-start | bytes 3145732
  33.2 5.4 %collective-permute-start.14 = (bf16[128,512]{1,0:T(8,128)(2,1)S(1)}, bf16[128,512]{1,0:T(8,128)(2,1)S(1)}, u32[]{:S(2)}, u32[]{:S(2)}) collective-permute-start(bf16[128,512]{1,0:T(8,128)(2,1)S(1)} %get-tuple-element.39), channel_id=1, source_target_pairs={{0,1},{1,0},{2,3},{3,2},{4,5},{5,4},{6,7},{7,6},{8,9},{9,8},{10,11... | collective-permute-start | bytes 393224 | tf_op jit(solution)/shard_map/ppermute | solution.py:175
  34.7 10.5 %collective-permute-start.15 = (bf16[128,512]{1,0:T(8,128)(2,1)S(1)}, bf16[128,512]{1,0:T(8,128)(2,1)S(1)}, u32[]{:S(2)}, u32[]{:S(2)}) collective-permute-start(bf16[128,512]{1,0:T(8,128)(2,1)S(1)} %get-tuple-element.40), channel_id=1, source_target_pairs={{0,2},{1,3},{2,0},{3,1},{4,6},{5,7},{6,4},{7,5},{8,10},{9,11},{10,... | collective-permute-start | bytes 393224 | tf_op jit(solution)/shard_map/ppermute | solution.py:175
  35.4 10.3 %collective-permute-start.16 = (bf16[128,512]{1,0:T(8,128)(2,1)S(1)}, bf16[128,512]{1,0:T(8,128)(2,1)S(1)}, u32[]{:S(2)}, u32[]{:S(2)}) collective-permute-start(bf16[128,512]{1,0:T(8,128)(2,1)S(1)} %get-tuple-element.41), channel_id=1, source_target_pairs={{0,3},{1,2},{2,1},{3,0},{4,7},{5,6},{6,5},{7,4},{8,11},{9,10},{10,... | collective-permute-start | bytes 393224 | tf_op jit(solution)/shard_map/ppermute | solution.py:175
  38.6 17.4 %collective-permute-start.22 = (bf16[256,256]{1,0:T(8,128)(2,1)S(1)}, bf16[256,256]{1,0:T(8,128)(2,1)S(1)}, u32[]{:S(2)}, u32[]{:S(2)}) collective-permute-start(bf16[256,256]{1,0:T(8,128)(2,1)S(1)} %get-tuple-element.43.h0), channel_id=1, source_target_pairs={{0,3},{1,2},{2,1},{3,0},{4,7},{5,6},{6,5},{7,4},{8,11},{9,10},{10,... | collective-permute-start | bytes 393224 | tf_op jit(solution)/shard_map/ppermute | solution.py:175
  45.2 4.5 %collective-permute-start.6 = (bf16[64,512]{1,0:T(8,128)(2,1)S(1)}, bf16[64,512]{1,0:T(8,128)(2,1)S(1)}, u32[]{:S(2)}, u32[]{:S(2)}) collective-permute-start(bf16[64,512]{1,0:T(8,128)(2,1)S(1)} %slice.80), channel_id=1, source_target_pairs={{0,8},{4,12},{8,0},{12,4},{16,24},{20,28},{24,16},{28,20},{1,9},{5... | collective-permute-start | bytes 196616 | tf_op jit(solution)/shard_map/ppermute | solution.py:175
  45.8 7.6 %collective-permute-start.17 = (bf16[64,512]{1,0:T(8,128)(2,1)S(1)}, bf16[64,512]{1,0:T(8,128)(2,1)S(1)}, u32[]{:S(2)}, u32[]{:S(2)}) collective-permute-start(bf16[64,512]{1,0:T(8,128)(2,1)S(1)} %get-tuple-element.47), channel_id=1, source_target_pairs={{0,16},{4,20},{8,24},{12,28},{16,0},{20,4},{24,8},{28,12},{1,17},{... | collective-permute-start | bytes 196616 | tf_op jit(solution)/shard_map/ppermute | solution.py:175
  49.8 6.1 %collective-permute-start.18 = (bf16[64,512]{1,0:T(8,128)(2,1)S(1)}, bf16[64,512]{1,0:T(8,128)(2,1)S(1)}, u32[]{:S(2)}, u32[]{:S(2)}) collective-permute-start(bf16[64,512]{1,0:T(8,128)(2,1)S(1)} %get-tuple-element.48), channel_id=1, source_target_pairs={{0,24},{4,28},{8,16},{12,20},{16,8},{20,12},{24,0},{28,4},{1,25},{... | collective-permute-start | bytes 196616 | tf_op jit(solution)/shard_map/ppermute | solution.py:175
  55.8 1.4 %collective-permute-start.19 = (bf16[128,512]{1,0:T(8,128)(2,1)S(1)}, bf16[128,512]{1,0:T(8,128)(2,1)S(1)}, u32[]{:S(2)}, u32[]{:S(2)}) collective-permute-start(bf16[128,512]{1,0:T(8,128)(2,1)S(1)} %pad_maximum_fusion.2), channel_id=1, source_target_pairs={{0,4},{4,0},{8,12},{12,8},{16,20},{20,16},{24,28},{28,24},{1,5},{5... | collective-permute-start | bytes 393224 | tf_op jit(solution)/shard_map/ppermute | solution.py:175

commit v3 on v2

--- a/solution.py
+++ b/solution.py
@@ -157,8 +157,8 @@
     val[...] = gate[...] * total
 
 
-def combine_body(own, other, comb, val, out):
-    x = jnp.concatenate([own[...], other[...]], axis=0)
+def combine_body(own, next_own, other, next_other, comb, val, out):
+    x = jnp.concatenate([r[...] for r in (own, next_own, other, next_other)], axis=0)
     n = x.shape[0]
     out[...] = (val[...] + dot(comb[:, :n], x) + dot(comb[:, n:], x)).astype(BF)
 
@@ -193,7 +193,8 @@
     w_gate, w_up, w_down = gate_proj[0], up_proj[0], down_proj[0]
     ff = w_gate.shape[1]
     near = (0, 1, 2, 3)
-    order = tuple(range(0, experts, 2)) + tuple(range(1, experts, 2))
+    own = (0, *range(4, experts, 2), 2)
+    order = own + tuple(r + 1 for r in own)
     far = tuple(range(4, experts, 2)) + tuple(range(5, experts, 2))
     fk = zs - 2
     dma = pltpu.SemaphoreType.DMA
@@ -266,13 +267,17 @@
     for i, k in enumerate(range(zs - 1, 1, -1)):
         back[k] = swap(sum_f[2 * slots * i : 2 * slots * (i + 1)], "ep", 2 * k)
     sum_n = reduce(near_part)
-    back[0] = sum_n[: 2 * slots]
-    back[1] = swap(sum_n[2 * slots :], "ep", 2)
-    mine = jnp.concatenate([back[k][:slots] for k in range(zs)], axis=0)
-    theirs = swap(jnp.concatenate([back[k][slots:] for k in range(zs)], axis=0), "ep", 1)
+    next_own, next_other = [], []
+    for at, k, got in ((2, 2, next_own), (3, 3, next_other)):
+        got.append(swap(sum_n[at * slots : (at + 1) * slots], "ep", k))
+    parts = [sum_n[: 2 * slots]] + [back[k] for k in range(2, zs)]
+    mine = jnp.concatenate([p[:slots] for p in parts], axis=0)
+    theirs = swap(jnp.concatenate([p[slots:] for p in parts], axis=0), "ep", 1)
 
     val = call(dense_out_body, shape((rows, width), F32), 8)(*hiddens, dense_out, side_gate)
-    return call(combine_body, shape((rows, width), BF), 8)(mine, theirs, comb, val)
+    return call(combine_body, shape((rows, width), BF), 8)(
+        mine, *next_own, theirs, *next_other, comb, val
+    )
 
 
 def general(

time: 58.4 us -> 53.4 us (0.914)
  starting transfers between devices: 32.1 us -> 29.4 us
  waiting for transfers between devices: 17.5 us -> 15.2 us
    ppermute x23 -> x24, starting transfers between devices: 32.1 us -> 29.4 us  [swap(): lax.ppermute(v, axis, [(i, i ^ k) for i in range(lax.axis_size(axis))])]
    ppermute x23 -> x24, waiting for transfers between devices: 17.5 us -> 15.2 us  [swap(): lax.ppermute(v, axis, [(i, i ^ k) for i in range(lax.axis_size(axis))])]
  transfers between devices with their start and end apart: 23 -> 24, of which waited for: 10 -> 7; matrix products, arithmetic and copies ran while one was open for 0% -> 0% of each run, Pallas kernels for 10% -> 11%
where the time goes in v3:
time: 53.4 us; the launch traced here: 53.3 us
  starting transfers between devices  29.4 us (55%)
  waiting for transfers between devices  15.2 us (28%)
  Pallas kernels  8.08 us (15%)
    ppermute x24, starting transfers between devices, swap(): lax.ppermute(v, axis, [(i, i ^ k) for i in range(lax.axis_size(axis))])  29.4 us
    ppermute x24, waiting for transfers between devices, swap(): lax.ppermute(v, axis, [(i, i ^ k) for i in range(lax.axis_size(axis))])  15.2 us
    pallas_call x1, Pallas kernels, fast(): call(near_body, (shape((4 * slots, width), BF),) * 4, 8)  1.87 us
    pallas_call x1, Pallas kernels, fast(): pl.pallas_call(functools.partial(pick_far_body, far), out_shape=(shape((f...  1.42 us
  transfers between devices with their start and end apart: 24, of which 7 were waited for; matrix products, arithmetic and copies ran while one was open for 0% of the time, Pallas kernels for 11%

profile of v3, /device:TPU:0, one launch (start us, length us, event | category | flops | bytes accessed | tf_op | source)
XLA Modules:
  0.0 53.3 jit_solution(1900495613800061394)
XLA Ops:
  0.0 1.4 %pick_far.1 = (bf16[64,1024]{1,0:T(8,128)(2,1)S(1)}, bf16[64,1024]{1,0:T(8,128)(2,1)S(1)}) custom-call(s32[8,32]{1,0:T(8,128)} %chosen.3, bf16[256,2048]{1,0:T(8,128)(2,1)} %tokens.5), custom_call_target="tpu_custom_call" | custom-call | flops 8000000000 | bytes 1048576 | tf_op jit(solution)/shard_map/pick_far/pallas_call | solution.py:202
  1.4 0.0 copy-start.5
  1.4 0.0 copy-start.8
  1.5 0.6 %collective-permute-start.6 = (bf16[64,1024]{1,0:T(8,128)(2,1)S(1)}, bf16[64,1024]{1,0:T(8,128)(2,1)S(1)}, u32[]{:S(2)}, u32[]{:S(2)}) collective-permute-start(bf16[64,1024]{1,0:T(8,128)(2,1)S(1)} %get-tuple-element.34), channel_id=1, source_target_pairs={{0,4},{4,0},{8,12},{12,8},{16,20},{20,16},{24,28},{28,24},{1,5},{5... | collective-permute-start | bytes 393224 | tf_op jit(solution)/shard_map/ppermute | solution.py:175
  2.0 0.4 shard_map.91
  2.5 0.1 collective-permute-start
  2.6 3.0 %collective-permute-start.1 = (bf16[32,2048]{1,0:T(8,128)(2,1)S(1)}, bf16[32,2048]{1,0:T(8,128)(2,1)S(1)}, u32[]{:S(2)}, u32[]{:S(2)}) collective-permute-start(bf16[32,2048]{1,0:T(8,128)(2,1)S(1)} %get-tuple-element.27), channel_id=1, source_target_pairs={{0,8},{4,12},{8,0},{12,4},{16,24},{20,28},{24,16},{28,20},{1,9},{5... | collective-permute-start | bytes 393224 | tf_op jit(solution)/shard_map/ppermute | solution.py:175
  5.6 0.0 copy-start
  5.6 0.0 copy-start.1
  5.6 0.0 copy-start.2
  5.7 0.5 shard_map.96
  6.2 1.6 %collective-permute-start.21 = (bf16[256,256]{1,0:T(8,128)(2,1)S(1)}, bf16[256,256]{1,0:T(8,128)(2,1)S(1)}, u32[]{:S(2)}, u32[]{:S(2)}) collective-permute-start(bf16[256,256]{1,0:T(8,128)(2,1)S(1)} %get-tuple-element.43.h0), channel_id=1, source_target_pairs={{0,1},{1,0},{2,3},{3,2},{4,5},{5,4},{6,7},{7,6},{8,9},{9,8},{10,11... | collective-permute-start | bytes 393224 | tf_op jit(solution)/shard_map/ppermute | solution.py:175
  7.8 3.5 %collective-permute-start.7 = (bf16[64,512]{1,0:T(8,128)(2,1)S(1)}, bf16[64,512]{1,0:T(8,128)(2,1)S(1)}, u32[]{:S(2)}, u32[]{:S(2)}) collective-permute-start(bf16[64,512]{1,0:T(8,128)(2,1)S(1)} %pad_maximum_fusion.3), channel_id=1, source_target_pairs={{0,24},{4,28},{8,16},{12,20},{16,8},{20,12},{24,0},{28,4},{1,25},{... | collective-permute-start | bytes 196616 | tf_op jit(solution)/shard_map/ppermute | solution.py:175
  11.3 1.6 %collective-permute-start.22 = (bf16[256,256]{1,0:T(8,128)(2,1)S(1)}, bf16[256,256]{1,0:T(8,128)(2,1)S(1)}, u32[]{:S(2)}, u32[]{:S(2)}) collective-permute-start(bf16[256,256]{1,0:T(8,128)(2,1)S(1)} %get-tuple-element.43.h0), channel_id=1, source_target_pairs={{0,2},{1,3},{2,0},{3,1},{4,6},{5,7},{6,4},{7,5},{8,10},{9,11},{10,... | collective-permute-start | bytes 393224 | tf_op jit(solution)/shard_map/ppermute | solution.py:175
  12.9 0.5 collective-permute-start.23
  13.4 2.4 %collective-permute-done.7 = bf16[64,512]{1,0:T(8,128)(2,1)S(1)} collective-permute-done((bf16[64,512]{1,0:T(8,128)(2,1)S(1)}, bf16[64,512]{1,0:T(8,128)(2,1)S(1)}, u32[]{:S(2)}, u32[]{:S(2)}) %collective-permute-start.7) | collective-permute-done | bytes 65568 | tf_op jit(solution)/shard_map/ppermute | solution.py:175
  15.7 0.0 collective-permute-start.8
  15.8 0.0 collective-permute-done.2.d
  15.8 1.8 %collective-permute-start.10 = (bf16[64,512]{1,0:T(8,128)(2,1)S(1)}, bf16[64,512]{1,0:T(8,128)(2,1)S(1)}, u32[]{:S(2)}, u32[]{:S(2)}) collective-permute-start(bf16[64,512]{1,0:T(8,128)(2,1)S(1)} %pad_maximum_fusion.5), channel_id=1, source_target_pairs={{0,24},{4,28},{8,16},{12,20},{16,8},{20,12},{24,0},{28,4},{1,25},{... | collective-permute-start | bytes 196616 | tf_op jit(solution)/shard_map/ppermute | solution.py:175
  17.6 5.0 %collective-permute-done.8 = bf16[64,512]{1,0:T(8,128)(2,1)S(1)} collective-permute-done((bf16[64,512]{1,0:T(8,128)(2,1)S(1)}, bf16[64,512]{1,0:T(8,128)(2,1)S(1)}, u32[]{:S(2)}, u32[]{:S(2)}) %collective-permute-start.8) | collective-permute-done | bytes 65568 | tf_op jit(solution)/shard_map/ppermute | solution.py:175
  22.6 0.0 collective-permute-done.21.h1
  22.6 2.0 %collective-permute-start.12 = (bf16[128,512]{1,0:T(8,128)(2,1)S(1)}, bf16[128,512]{1,0:T(8,128)(2,1)S(1)}, u32[]{:S(2)}, u32[]{:S(2)}) collective-permute-start(bf16[128,512]{1,0:T(8,128)(2,1)S(1)} %constant_dynamic-update-slice_fusion.c0), channel_id=1, source_target_pairs={{0,1},{1,0},{2,3},{3,2},{4,5},{5,4},{6,7},{7,6},{8,9},{9,8},{10,11... | collective-permute-start | bytes 393224 | tf_op jit(solution)/shard_map/ppermute | solution.py:175
  24.6 1.5 %collective-permute-start.9 = (bf16[128,512]{1,0:T(8,128)(2,1)S(1)}, bf16[128,512]{1,0:T(8,128)(2,1)S(1)}, u32[]{:S(2)}, u32[]{:S(2)}) collective-permute-start(bf16[128,512]{1,0:T(8,128)(2,1)S(1)} %constant_dynamic-update-slice_fusion.c0), channel_id=1, source_target_pairs={{0,2},{1,3},{2,0},{3,1},{4,6},{5,7},{6,4},{7,5},{8,10},{9,11},{10,... | collective-permute-start | bytes 393224 | tf_op jit(solution)/shard_map/ppermute | solution.py:175
  26.2 1.9 %shard_map.92 = (bf16[128,512]{1,0:T(8,128)(2,1)S(1)}, bf16[128,512]{1,0:T(8,128)(2,1)S(1)}, bf16[128,512]{1,0:T(8,128)(2,1)S(1)}, bf16[128,512]{1,0:T(8,128)(2,1)S(1)}) custom-call(bf16[32,2048]{1,0:T(8,128)(2,1)S(1)} %get-tuple-element.25.a, bf16[32,2048]{1,0:T(8,128)(2,1)S(1)} %collective-permute-done.b, bf16[32,2048]{1,0:T(8,128)(2,1)S(1)} %collective-permute-done.1.c, ...), custom_call_target="tpu_custom_call" | custom-call | tf_op jit(solution)/shard_map/pallas_call | solution.py:247
  28.0 0.0 collective-permute-done.23.h3
  28.1 0.1 collective-permute-start.3
  28.2 0.5 collective-permute-start.4
  28.7 2.9 %collective-permute-start.5 = (bf16[128,512]{1,0:T(8,128)(2,1)S(1)}, bf16[128,512]{1,0:T(8,128)(2,1)S(1)}, u32[]{:S(2)}, u32[]{:S(2)}) collective-permute-start(bf16[128,512]{1,0:T(8,128)(2,1)S(1)} %get-tuple-element.32), channel_id=1, source_target_pairs={{0,3},{1,2},{2,1},{3,0},{4,7},{5,6},{6,5},{7,4},{8,11},{9,10},{10,... | collective-permute-start | bytes 393224 | tf_op jit(solution)/shard_map/ppermute | solution.py:175
  31.6 0.4 shard_map.97.val
  32.1 0.7 %shard_map.93 = (f32[128,1024]{1,0:T(8,128)S(1)}, f32[128,1024]{1,0:T(8,128)S(1)}) custom-call(bf16[128,512]{1,0:T(8,128)(2,1)S(1)} %constant_dynamic-update-slice_fusion.c0, bf16[128,512]{1,0:T(8,128)(2,1)S(1)} %collective-permute-done.12.c1, bf16[2048,1024]{1,0:T(8,128)(2,1)S(1)} %bitcast.8, bf16[2048,1024]{1,0:T(8,128)(2,1)S(1)} %bitcast.11, ...), custom_call_target="tpu_custom_call" | custom-call | tf_op jit(solution)/shard_map/pallas_call | solution.py:251
  32.9 1.1 %shard_map.94 = (bf16[128,1024]{1,0:T(8,128)(2,1)S(1)}, bf16[128,512]{1,0:T(8,128)(2,1)S(1)}) custom-call(bf16[128,512]{1,0:T(8,128)(2,1)S(1)} %collective-permute-done.9.c2, bf16[128,512]{1,0:T(8,128)(2,1)S(1)} %pad_maximum_fusion.c3, f32[128,1024]{1,0:T(8,128)S(1)} %get-tuple-element.35.acc_gate, f32[128,1024]{1,0:T(8,128)S(1)} %get-tuple-element.36.acc_up, ...), custom_call_target="tpu_custom_call" | custom-call | tf_op jit(solution)/shard_map/pallas_call | solution.py:254
  33.9 0.6 %shard_map.95 = (bf16[128,512]{1,0:T(8,128)(2,1)S(1)}, bf16[128,512]{1,0:T(8,128)(2,1)S(1)}, bf16[128,512]{1,0:T(8,128)(2,1)S(1)}) custom-call(bf16[128,1024]{1,0:T(8,128)(2,1)S(1)} %get-tuple-element.37.hidden, bf16[1024,2048]{1,0:T(8,128)(2,1)S(1)} %bitcast.6), custom_call_target="tpu_custom_call" | custom-call | tf_op jit(solution)/shard_map/pallas_call | solution.py:257
  34.5 0.1 collective-permute-start.13
  34.6 0.5 %collective-permute-start.14 = (bf16[128,512]{1,0:T(8,128)(2,1)S(1)}, bf16[128,512]{1,0:T(8,128)(2,1)S(1)}, u32[]{:S(2)}, u32[]{:S(2)}) collective-permute-start(bf16[128,512]{1,0:T(8,128)(2,1)S(1)} %get-tuple-element.40), channel_id=1, source_target_pairs={{0,2},{1,3},{2,0},{3,1},{4,6},{5,7},{6,4},{7,5},{8,10},{9,11},{10,... | collective-permute-start | bytes 393224 | tf_op jit(solution)/shard_map/ppermute | solution.py:175
  35.2 2.9 %collective-permute-start.15 = (bf16[128,512]{1,0:T(8,128)(2,1)S(1)}, bf16[128,512]{1,0:T(8,128)(2,1)S(1)}, u32[]{:S(2)}, u32[]{:S(2)}) collective-permute-start(bf16[128,512]{1,0:T(8,128)(2,1)S(1)} %get-tuple-element.41), channel_id=1, source_target_pairs={{0,3},{1,2},{2,1},{3,0},{4,7},{5,6},{6,5},{7,4},{8,11},{9,10},{10,... | collective-permute-start | bytes 393224 | tf_op jit(solution)/shard_map/ppermute | solution.py:175
  38.1 0.1 add_convert_fusion.1
  38.2 1.4 %collective-permute-done.13 = bf16[128,512]{1,0:T(8,128)(2,1)S(1)} collective-permute-done((bf16[128,512]{1,0:T(8,128)(2,1)S(1)}, bf16[128,512]{1,0:T(8,128)(2,1)S(1)}, u32[]{:S(2)}, u32[]{:S(2)}) %collective-permute-start.13) | collective-permute-done | bytes 131104 | tf_op jit(solution)/shard_map/ppermute | solution.py:175
  39.6 0.1 collective-permute-done.14
  39.6 1.4 %collective-permute-done.15 = bf16[128,512]{1,0:T(8,128)(2,1)S(1)} collective-permute-done((bf16[128,512]{1,0:T(8,128)(2,1)S(1)}, bf16[128,512]{1,0:T(8,128)(2,1)S(1)}, u32[]{:S(2)}, u32[]{:S(2)}) %collective-permute-start.15) | collective-permute-done | bytes 131104 | tf_op jit(solution)/shard_map/ppermute | solution.py:175
  41.1 0.1 add_convert_fusion
  41.1 3.0 %collective-permute-start.16 = (bf16[64,512]{1,0:T(8,128)(2,1)S(1)}, bf16[64,512]{1,0:T(8,128)(2,1)S(1)}, u32[]{:S(2)}, u32[]{:S(2)}) collective-permute-start(bf16[64,512]{1,0:T(8,128)(2,1)S(1)} %get-tuple-element.49), channel_id=1, source_target_pairs={{0,16},{4,20},{8,24},{12,28},{16,0},{20,4},{24,8},{28,12},{1,17},{... | collective-permute-start | bytes 196616 | tf_op jit(solution)/shard_map/ppermute | solution.py:175
  44.1 0.1 collective-permute-start.18
  44.2 0.1 collective-permute-start.20
  44.3 2.1 %collective-permute-start.17 = (bf16[64,512]{1,0:T(8,128)(2,1)S(1)}, bf16[64,512]{1,0:T(8,128)(2,1)S(1)}, u32[]{:S(2)}, u32[]{:S(2)}) collective-permute-start(bf16[64,512]{1,0:T(8,128)(2,1)S(1)} %get-tuple-element.50), channel_id=1, source_target_pairs={{0,24},{4,28},{8,16},{12,20},{16,8},{20,12},{24,0},{28,4},{1,25},{... | collective-permute-start | bytes 196616 | tf_op jit(solution)/shard_map/ppermute | solution.py:175
  46.4 4.1 %collective-permute-done.17 = bf16[64,512]{1,0:T(8,128)(2,1)S(1)} collective-permute-done((bf16[64,512]{1,0:T(8,128)(2,1)S(1)}, bf16[64,512]{1,0:T(8,128)(2,1)S(1)}, u32[]{:S(2)}, u32[]{:S(2)}) %collective-permute-start.17) | collective-permute-done | bytes 65568 | tf_op jit(solution)/shard_map/ppermute | solution.py:175
  50.5 0.8 %collective-permute-start.19 = (bf16[96,512]{1,0:T(8,128)(2,1)S(1)}, bf16[96,512]{1,0:T(8,128)(2,1)S(1)}, u32[]{:S(2)}, u32[]{:S(2)}) collective-permute-start(bf16[96,512]{1,0:T(8,128)(2,1)S(1)} %pad_maximum_fusion.2), channel_id=1, source_target_pairs={{0,4},{4,0},{8,12},{12,8},{16,20},{20,16},{24,28},{28,24},{1,5},{5... | collective-permute-start | bytes 294920 | tf_op jit(solution)/shard_map/ppermute | solution.py:175
  51.4 0.9 %collective-permute-done.19.other = bf16[96,512]{1,0:T(8,128)(2,1)S(1)} collective-permute-done((bf16[96,512]{1,0:T(8,128)(2,1)S(1)}, bf16[96,512]{1,0:T(8,128)(2,1)S(1)}, u32[]{:S(2)}, u32[]{:S(2)}) %collective-permute-start.19) | collective-permute-done | bytes 98336 | tf_op jit(solution)/shard_map/ppermute | solution.py:175
  52.3 1.0 %shard_map.98 = bf16[256,512]{1,0:T(8,128)(2,1)} custom-call(bf16[96,512]{1,0:T(8,128)(2,1)S(1)} %pad_maximum_fusion.1.own, bf16[32,512]{1,0:T(8,128)(2,1)S(1)} %collective-permute-done.18.next_own, bf16[96,512]{1,0:T(8,128)(2,1)S(1)} %collective-permute-done.19.other, bf16[32,512]{1,0:T(8,128)(2,1)S(1)} %collective-permute-done.20.next_other, ...), custom_call_target="tpu_custom_call" | custom-call | tf_op jit(solution)/shard_map/pallas_call | solution.py:278
  (44 shorter events, 0.2 us)
Async XLA Ops:
  0.0 2.0 %copy-start.6 = (s32[8,32]{1,0:T(8,128)S(1)}, s32[8,32]{1,0:T(8,128)}, u32[]{:S(2)}) copy-start(s32[8,32]{1,0:T(8,128)} %chosen.3) | copy-start | bytes 3076
  0.0 2.0 %copy-start.4 = (bf16[256,2048]{1,0:T(8,128)(2,1)S(1)}, bf16[256,2048]{1,0:T(8,128)(2,1)}, u32[]{:S(2)}) copy-start(bf16[256,2048]{1,0:T(8,128)(2,1)} %tokens.5) | copy-start | bytes 3145732
  0.0 2.0 %copy-start.7 = (f32[8,32]{1,0:T(8,128)S(1)}, f32[8,32]{1,0:T(8,128)}, u32[]{:S(2)}) copy-start(f32[8,32]{1,0:T(8,128)} %weights.1) | copy-start | bytes 3076
  1.4 4.2 %copy-start.5 = (bf16[2048,256]{1,0:T(8,128)(2,1)S(1)}, bf16[2048,256]{1,0:T(8,128)(2,1)}, u32[]{:S(2)}) copy-start(bf16[2048,256]{1,0:T(8,128)(2,1)} %w_in.1) | copy-start | bytes 3145732
  1.4 4.2 %copy-start.8 = (bf16[2048]{0:T(1024)(128)(2,1)S(1)}, bf16[2048]{0:T(1024)(128)(2,1)}, u32[]{:S(2)}) copy-start(bf16[2048]{0:T(1024)(128)(2,1)} %w_gate.1) | copy-start | bytes 12292
  1.5 6.3 %collective-permute-start.6 = (bf16[64,1024]{1,0:T(8,128)(2,1)S(1)}, bf16[64,1024]{1,0:T(8,128)(2,1)S(1)}, u32[]{:S(2)}, u32[]{:S(2)}) collective-permute-start(bf16[64,1024]{1,0:T(8,128)(2,1)S(1)} %get-tuple-element.34), channel_id=1, source_target_pairs={{0,4},{4,0},{8,12},{12,8},{16,20},{20,16},{24,28},{28,24},{1,5},{5... | collective-permute-start | bytes 393224 | tf_op jit(solution)/shard_map/ppermute | solution.py:175
  2.5 8.8 %collective-permute-start = (bf16[32,2048]{1,0:T(8,128)(2,1)S(1)}, bf16[32,2048]{1,0:T(8,128)(2,1)S(1)}, u32[]{:S(2)}, u32[]{:S(2)}) collective-permute-start(bf16[32,2048]{1,0:T(8,128)(2,1)S(1)} %get-tuple-element.26), channel_id=1, source_target_pairs={{0,4},{4,0},{8,12},{12,8},{16,20},{20,16},{24,28},{28,24},{1,5},{5... | collective-permute-start | bytes 393224 | tf_op jit(solution)/shard_map/ppermute | solution.py:175
  2.6 10.3 %collective-permute-start.1 = (bf16[32,2048]{1,0:T(8,128)(2,1)S(1)}, bf16[32,2048]{1,0:T(8,128)(2,1)S(1)}, u32[]{:S(2)}, u32[]{:S(2)}) collective-permute-start(bf16[32,2048]{1,0:T(8,128)(2,1)S(1)} %get-tuple-element.27), channel_id=1, source_target_pairs={{0,8},{4,12},{8,0},{12,4},{16,24},{20,28},{24,16},{28,20},{1,9},{5... | collective-permute-start | bytes 393224 | tf_op jit(solution)/shard_map/ppermute | solution.py:175
  5.6 10.2 %collective-permute-start.2 = (bf16[32,2048]{1,0:T(8,128)(2,1)S(1)}, bf16[32,2048]{1,0:T(8,128)(2,1)S(1)}, u32[]{:S(2)}, u32[]{:S(2)}) collective-permute-start(bf16[32,2048]{1,0:T(8,128)(2,1)S(1)} %get-tuple-element.28), channel_id=1, source_target_pairs={{0,12},{4,8},{8,4},{12,0},{16,28},{20,24},{24,20},{28,16},{1,13},{... | collective-permute-start | bytes 393224 | tf_op jit(solution)/shard_map/ppermute | solution.py:175
  5.6 20.5 %copy-start = (bf16[1,1024,2048]{2,1,0:T(8,128)(2,1)S(1)}, bf16[1,1024,2048]{2,1,0:T(8,128)(2,1)}, u32[]{:S(2)}) copy-start(bf16[1,1024,2048]{2,1,0:T(8,128)(2,1)} %param.12) | copy-start | bytes 12582916
  5.6 20.5 %copy-start.1 = (bf16[1,2048,1024]{2,1,0:T(8,128)(2,1)S(1)}, bf16[1,2048,1024]{2,1,0:T(8,128)(2,1)}, u32[]{:S(2)}) copy-start(bf16[1,2048,1024]{2,1,0:T(8,128)(2,1)} %param.10) | copy-start | bytes 12582916
  5.6 20.5 %copy-start.2 = (bf16[1,2048,1024]{2,1,0:T(8,128)(2,1)S(1)}, bf16[1,2048,1024]{2,1,0:T(8,128)(2,1)}, u32[]{:S(2)}) copy-start(bf16[1,2048,1024]{2,1,0:T(8,128)(2,1)} %param.11) | copy-start | bytes 12582916
  6.2 16.4 %collective-permute-start.21 = (bf16[256,256]{1,0:T(8,128)(2,1)S(1)}, bf16[256,256]{1,0:T(8,128)(2,1)S(1)}, u32[]{:S(2)}, u32[]{:S(2)}) collective-permute-start(bf16[256,256]{1,0:T(8,128)(2,1)S(1)} %get-tuple-element.43.h0), channel_id=1, source_target_pairs={{0,1},{1,0},{2,3},{3,2},{4,5},{5,4},{6,7},{7,6},{8,9},{9,8},{10,11... | collective-permute-start | bytes 393224 | tf_op jit(solution)/shard_map/ppermute | solution.py:175
  7.8 8.0 %collective-permute-start.7 = (bf16[64,512]{1,0:T(8,128)(2,1)S(1)}, bf16[64,512]{1,0:T(8,128)(2,1)S(1)}, u32[]{:S(2)}, u32[]{:S(2)}) collective-permute-start(bf16[64,512]{1,0:T(8,128)(2,1)S(1)} %pad_maximum_fusion.3), channel_id=1, source_target_pairs={{0,24},{4,28},{8,16},{12,20},{16,8},{20,12},{24,0},{28,4},{1,25},{... | collective-permute-start | bytes 196616 | tf_op jit(solution)/shard_map/ppermute | solution.py:175
  11.3 13.3 %collective-permute-start.22 = (bf16[256,256]{1,0:T(8,128)(2,1)S(1)}, bf16[256,256]{1,0:T(8,128)(2,1)S(1)}, u32[]{:S(2)}, u32[]{:S(2)}) collective-permute-start(bf16[256,256]{1,0:T(8,128)(2,1)S(1)} %get-tuple-element.43.h0), channel_id=1, source_target_pairs={{0,2},{1,3},{2,0},{3,1},{4,6},{5,7},{6,4},{7,5},{8,10},{9,11},{10,... | collective-permute-start | bytes 393224 | tf_op jit(solution)/shard_map/ppermute | solution.py:175
  12.9 15.1 %collective-permute-start.23 = (bf16[256,256]{1,0:T(8,128)(2,1)S(1)}, bf16[256,256]{1,0:T(8,128)(2,1)S(1)}, u32[]{:S(2)}, u32[]{:S(2)}) collective-permute-start(bf16[256,256]{1,0:T(8,128)(2,1)S(1)} %get-tuple-element.43.h0), channel_id=1, source_target_pairs={{0,3},{1,2},{2,1},{3,0},{4,7},{5,6},{6,5},{7,4},{8,11},{9,10},{10,... | collective-permute-start | bytes 393224 | tf_op jit(solution)/shard_map/ppermute | solution.py:175
  15.7 6.8 %collective-permute-start.8 = (bf16[64,512]{1,0:T(8,128)(2,1)S(1)}, bf16[64,512]{1,0:T(8,128)(2,1)S(1)}, u32[]{:S(2)}, u32[]{:S(2)}) collective-permute-start(bf16[64,512]{1,0:T(8,128)(2,1)S(1)} %pad_maximum_fusion.4), channel_id=1, source_target_pairs={{0,16},{4,20},{8,24},{12,28},{16,0},{20,4},{24,8},{28,12},{1,17},{... | collective-permute-start | bytes 196616 | tf_op jit(solution)/shard_map/ppermute | solution.py:175
  15.8 12.4 %collective-permute-start.10 = (bf16[64,512]{1,0:T(8,128)(2,1)S(1)}, bf16[64,512]{1,0:T(8,128)(2,1)S(1)}, u32[]{:S(2)}, u32[]{:S(2)}) collective-permute-start(bf16[64,512]{1,0:T(8,128)(2,1)S(1)} %pad_maximum_fusion.5), channel_id=1, source_target_pairs={{0,24},{4,28},{8,16},{12,20},{16,8},{20,12},{24,0},{28,4},{1,25},{... | collective-permute-start | bytes 196616 | tf_op jit(solution)/shard_map/ppermute | solution.py:175
  22.6 6.2 %collective-permute-start.11 = (bf16[64,512]{1,0:T(8,128)(2,1)S(1)}, bf16[64,512]{1,0:T(8,128)(2,1)S(1)}, u32[]{:S(2)}, u32[]{:S(2)}) collective-permute-start(bf16[64,512]{1,0:T(8,128)(2,1)S(1)} %pad_maximum_fusion.6), channel_id=1, source_target_pairs={{0,16},{4,20},{8,24},{12,28},{16,0},{20,4},{24,8},{28,12},{1,17},{... | collective-permute-start | bytes 196616 | tf_op jit(solution)/shard_map/ppermute | solution.py:175
  22.6 9.5 %collective-permute-start.12 = (bf16[128,512]{1,0:T(8,128)(2,1)S(1)}, bf16[128,512]{1,0:T(8,128)(2,1)S(1)}, u32[]{:S(2)}, u32[]{:S(2)}) collective-permute-start(bf16[128,512]{1,0:T(8,128)(2,1)S(1)} %constant_dynamic-update-slice_fusion.c0), channel_id=1, source_target_pairs={{0,1},{1,0},{2,3},{3,2},{4,5},{5,4},{6,7},{7,6},{8,9},{9,8},{10,11... | collective-permute-start | bytes 393224 | tf_op jit(solution)/shard_map/ppermute | solution.py:175
  24.6 8.2 %collective-permute-start.9 = (bf16[128,512]{1,0:T(8,128)(2,1)S(1)}, bf16[128,512]{1,0:T(8,128)(2,1)S(1)}, u32[]{:S(2)}, u32[]{:S(2)}) collective-permute-start(bf16[128,512]{1,0:T(8,128)(2,1)S(1)} %constant_dynamic-update-slice_fusion.c0), channel_id=1, source_target_pairs={{0,2},{1,3},{2,0},{3,1},{4,6},{5,7},{6,4},{7,5},{8,10},{9,11},{10,... | collective-permute-start | bytes 393224 | tf_op jit(solution)/shard_map/ppermute | solution.py:175
  26.2 5.5 %copy-start.3 = (bf16[1024,512]{1,0:T(8,128)(2,1)S(1)}, bf16[1024,512]{1,0:T(8,128)(2,1)}, u32[]{:S(2)}) copy-start(bf16[1024,512]{1,0:T(8,128)(2,1)} %w_out.1) | copy-start | bytes 3145732
  28.1 7.1 %collective-permute-start.3 = (bf16[128,512]{1,0:T(8,128)(2,1)S(1)}, bf16[128,512]{1,0:T(8,128)(2,1)S(1)}, u32[]{:S(2)}, u32[]{:S(2)}) collective-permute-start(bf16[128,512]{1,0:T(8,128)(2,1)S(1)} %get-tuple-element.30), channel_id=1, source_target_pairs={{0,1},{1,0},{2,3},{3,2},{4,5},{5,4},{6,7},{7,6},{8,9},{9,8},{10,11... | collective-permute-start | bytes 393224 | tf_op jit(solution)/shard_map/ppermute | solution.py:175
  28.2 9.9 %collective-permute-start.4 = (bf16[128,512]{1,0:T(8,128)(2,1)S(1)}, bf16[128,512]{1,0:T(8,128)(2,1)S(1)}, u32[]{:S(2)}, u32[]{:S(2)}) collective-permute-start(bf16[128,512]{1,0:T(8,128)(2,1)S(1)} %get-tuple-element.31), channel_id=1, source_target_pairs={{0,2},{1,3},{2,0},{3,1},{4,6},{5,7},{6,4},{7,5},{8,10},{9,11},{10,... | collective-permute-start | bytes 393224 | tf_op jit(solution)/shard_map/ppermute | solution.py:175
  28.7 9.4 %collective-permute-start.5 = (bf16[128,512]{1,0:T(8,128)(2,1)S(1)}, bf16[128,512]{1,0:T(8,128)(2,1)S(1)}, u32[]{:S(2)}, u32[]{:S(2)}) collective-permute-start(bf16[128,512]{1,0:T(8,128)(2,1)S(1)} %get-tuple-element.32), channel_id=1, source_target_pairs={{0,3},{1,2},{2,1},{3,0},{4,7},{5,6},{6,5},{7,4},{8,11},{9,10},{10,... | collective-permute-start | bytes 393224 | tf_op jit(solution)/shard_map/ppermute | solution.py:175
  34.5 5.0 %collective-permute-start.13 = (bf16[128,512]{1,0:T(8,128)(2,1)S(1)}, bf16[128,512]{1,0:T(8,128)(2,1)S(1)}, u32[]{:S(2)}, u32[]{:S(2)}) collective-permute-start(bf16[128,512]{1,0:T(8,128)(2,1)S(1)} %get-tuple-element.39), channel_id=1, source_target_pairs={{0,1},{1,0},{2,3},{3,2},{4,5},{5,4},{6,7},{7,6},{8,9},{9,8},{10,11... | collective-permute-start | bytes 393224 | tf_op jit(solution)/shard_map/ppermute | solution.py:175
  34.6 5.0 %collective-permute-start.14 = (bf16[128,512]{1,0:T(8,128)(2,1)S(1)}, bf16[128,512]{1,0:T(8,128)(2,1)S(1)}, u32[]{:S(2)}, u32[]{:S(2)}) collective-permute-start(bf16[128,512]{1,0:T(8,128)(2,1)S(1)} %get-tuple-element.40), channel_id=1, source_target_pairs={{0,2},{1,3},{2,0},{3,1},{4,6},{5,7},{6,4},{7,5},{8,10},{9,11},{10,... | collective-permute-start | bytes 393224 | tf_op jit(solution)/shard_map/ppermute | solution.py:175
  35.2 5.9 %collective-permute-start.15 = (bf16[128,512]{1,0:T(8,128)(2,1)S(1)}, bf16[128,512]{1,0:T(8,128)(2,1)S(1)}, u32[]{:S(2)}, u32[]{:S(2)}) collective-permute-start(bf16[128,512]{1,0:T(8,128)(2,1)S(1)} %get-tuple-element.41), channel_id=1, source_target_pairs={{0,3},{1,2},{2,1},{3,0},{4,7},{5,6},{6,5},{7,4},{8,11},{9,10},{10,... | collective-permute-start | bytes 393224 | tf_op jit(solution)/shard_map/ppermute | solution.py:175
  41.1 5.3 %collective-permute-start.16 = (bf16[64,512]{1,0:T(8,128)(2,1)S(1)}, bf16[64,512]{1,0:T(8,128)(2,1)S(1)}, u32[]{:S(2)}, u32[]{:S(2)}) collective-permute-start(bf16[64,512]{1,0:T(8,128)(2,1)S(1)} %get-tuple-element.49), channel_id=1, source_target_pairs={{0,16},{4,20},{8,24},{12,28},{16,0},{20,4},{24,8},{28,12},{1,17},{... | collective-permute-start | bytes 196616 | tf_op jit(solution)/shard_map/ppermute | solution.py:175
  44.1 7.2 %collective-permute-start.18 = (bf16[32,512]{1,0:T(8,128)(2,1)S(1)}, bf16[32,512]{1,0:T(8,128)(2,1)S(1)}, u32[]{:S(2)}, u32[]{:S(2)}) collective-permute-start(bf16[32,512]{1,0:T(8,128)(2,1)S(1)} %get-tuple-element.47), channel_id=1, source_target_pairs={{0,8},{4,12},{8,0},{12,4},{16,24},{20,28},{24,16},{28,20},{1,9},{5... | collective-permute-start | bytes 98312 | tf_op jit(solution)/shard_map/ppermute | solution.py:175
  44.2 7.1 %collective-permute-start.20 = (bf16[32,512]{1,0:T(8,128)(2,1)S(1)}, bf16[32,512]{1,0:T(8,128)(2,1)S(1)}, u32[]{:S(2)}, u32[]{:S(2)}) collective-permute-start(bf16[32,512]{1,0:T(8,128)(2,1)S(1)} %get-tuple-element.45), channel_id=1, source_target_pairs={{0,12},{4,8},{8,4},{12,0},{16,28},{20,24},{24,20},{28,16},{1,13},{... | collective-permute-start | bytes 98312 | tf_op jit(solution)/shard_map/ppermute | solution.py:175
  44.3 6.2 %collective-permute-start.17 = (bf16[64,512]{1,0:T(8,128)(2,1)S(1)}, bf16[64,512]{1,0:T(8,128)(2,1)S(1)}, u32[]{:S(2)}, u32[]{:S(2)}) collective-permute-start(bf16[64,512]{1,0:T(8,128)(2,1)S(1)} %get-tuple-element.50), channel_id=1, source_target_pairs={{0,24},{4,28},{8,16},{12,20},{16,8},{20,12},{24,0},{28,4},{1,25},{... | collective-permute-start | bytes 196616 | tf_op jit(solution)/shard_map/ppermute | solution.py:175
  50.5 1.7 %collective-permute-start.19 = (bf16[96,512]{1,0:T(8,128)(2,1)S(1)}, bf16[96,512]{1,0:T(8,128)(2,1)S(1)}, u32[]{:S(2)}, u32[]{:S(2)}) collective-permute-start(bf16[96,512]{1,0:T(8,128)(2,1)S(1)} %pad_maximum_fusion.2), channel_id=1, source_target_pairs={{0,4},{4,0},{8,12},{12,8},{16,20},{20,16},{24,28},{28,24},{1,5},{5... | collective-permute-start | bytes 294920 | tf_op jit(solution)/shard_map/ppermute | solution.py:175

commit v4 on v3

--- a/solution.py
+++ b/solution.py
@@ -133,21 +133,10 @@
     down((silu(gate) * up).astype(BF), w_down, ((3, p3), (1, p1), (2, p2), (0, p0)))
 
 
-def far_a_body(c0, c1, w_gate, w_up, w_down, acc_gate, acc_up):
-    del w_down
-    acc_gate[...], acc_up[...] = enter(((0, c0), (1, c1)), w_gate, w_up)
-
-
-def far_b_body(c2, c3, acc_gate, acc_up, w_gate, w_up, w_down, hidden, p3):
-    gate, up = enter(((2, c2), (3, c3)), w_gate, w_up)
-    gate, up = gate + acc_gate[...], up + acc_up[...]
+def far_body(c0, c1, c2, c3, w_gate, w_up, w_down, p0, p1, p2, p3):
+    gate, up = enter(((0, c0), (1, c1), (2, c2), (3, c3)), w_gate, w_up)
     h = (silu(gate) * up).astype(BF)
-    hidden[...] = h
-    down(h, w_down, ((3, p3),))
-
-
-def far_c_body(hidden, w_down, p0, p1, p2):
-    down(hidden[...], w_down, ((1, p1), (2, p2), (0, p0)))
+    down(h, w_down, ((3, p3), (1, p1), (2, p2), (0, p0)))
 
 
 def dense_out_body(h0, h1, h2, h3, w_out, gate, val):
@@ -191,7 +180,6 @@
     width = model // lax.axis_size("tp")
     zs = experts // 2
     w_gate, w_up, w_down = gate_proj[0], up_proj[0], down_proj[0]
-    ff = w_gate.shape[1]
     near = (0, 1, 2, 3)
     own = (0, *range(4, experts, 2), 2)
     order = own + tuple(r + 1 for r in own)
@@ -248,14 +236,9 @@
         keep_n, got_n, z1a, z1b, w_gate, w_up, w_down
     )
     far_rows = 2 * fk * slots
-    accs = call(far_a_body, (shape((far_rows, ff), F32),) * 2, 8)(
-        chunks[0], chunks[1], w_gate, w_up, w_down
-    )
-    hidden, part3 = call(
-        far_b_body, (shape((far_rows, ff), BF), shape((far_rows, width), BF)), 8
-    )(chunks[2], waves[1], *accs, w_gate, w_up, w_down)
-    far_part = call(far_c_body, (shape((far_rows, width), BF),) * 3, 8)(hidden, w_down)
-    far_part = [*far_part, part3]
+    far_part = call(far_body, (shape((far_rows, width), BF),) * 4, 8)(
+        *chunks, waves[1], w_gate, w_up, w_down
+    )
 
     def reduce(part):
         sent = exchange(part)
@@ -274,7 +257,9 @@
     mine = jnp.concatenate([p[:slots] for p in parts], axis=0)
     theirs = swap(jnp.concatenate([p[slots:] for p in parts], axis=0), "ep", 1)
 
-    val = call(dense_out_body, shape((rows, width), F32), 8)(*hiddens, dense_out, side_gate)
+    val = call(dense_out_body, shape((rows, width), F32), 8)(
+        *hiddens, dense_out, side_gate
+    )
     return call(combine_body, shape((rows, width), BF), 8)(
         mine, *next_own, theirs, *next_other, comb, val
     )

time: 53.4 us -> 55.5 us (1.039)
  starting transfers between devices: 29.4 us -> 30.9 us
  waiting for transfers between devices: 15.2 us -> 16.2 us
    ppermute x24, starting transfers between devices: 29.4 us -> 30.9 us  [swap(): lax.ppermute(v, axis, [(i, i ^ k) for i in range(lax.axis_size(axis))])]
    ppermute x24, waiting for transfers between devices: 15.2 us -> 16.2 us  [swap(): lax.ppermute(v, axis, [(i, i ^ k) for i in range(lax.axis_size(axis))])]
    pallas_call x3 -> x1, Pallas kernels: 2.41 us -> 1.96 us  [fast(): call(far_body, (shape((far_rows, width), BF),) * 4, 8)]
  transfers between devices with their start and end apart: 24 -> 24, of which waited for: 7 -> 8; matrix products, arithmetic and copies ran while one was open for 0% -> 0% of each run, Pallas kernels for 11% -> 9%
where the time goes in v4:
time: 55.5 us; the launch traced here: 55.4 us
  starting transfers between devices  30.9 us (56%)
  waiting for transfers between devices  16.2 us (29%)
  Pallas kernels  7.68 us (14%)
    ppermute x24, starting transfers between devices, swap(): lax.ppermute(v, axis, [(i, i ^ k) for i in range(lax.axis_size(axis))])  30.9 us
    ppermute x24, waiting for transfers between devices, swap(): lax.ppermute(v, axis, [(i, i ^ k) for i in range(lax.axis_size(axis))])  16.2 us
    pallas_call x1, Pallas kernels, fast(): call(far_body, (shape((far_rows, width), BF),) * 4, 8)  1.96 us
    pallas_call x1, Pallas kernels, fast(): call(near_body, (shape((4 * slots, width), BF),) * 4, 8)  1.91 us
    pallas_call x1, Pallas kernels, fast(): pl.pallas_call(functools.partial(pick_far_body, far), out_shape=(shape((f...  1.42 us
  transfers between devices with their start and end apart: 24, of which 8 were waited for; matrix products, arithmetic and copies ran while one was open for 0% of the time, Pallas kernels for 9%

profile of v4, /device:TPU:0, one launch (start us, length us, event | category | flops | bytes accessed | tf_op | source)
XLA Modules:
  0.0 55.4 jit_solution(14518256346264433450)
XLA Ops:
  0.0 1.4 %pick_far.1 = (bf16[64,1024]{1,0:T(8,128)(2,1)S(1)}, bf16[64,1024]{1,0:T(8,128)(2,1)S(1)}) custom-call(s32[8,32]{1,0:T(8,128)} %chosen.3, bf16[256,2048]{1,0:T(8,128)(2,1)} %tokens.5), custom_call_target="tpu_custom_call" | custom-call | flops 8000000000 | bytes 1048576 | tf_op jit(solution)/shard_map/pick_far/pallas_call | solution.py:190
  1.4 0.0 copy-start.5
  1.4 0.0 copy-start.8
  1.5 0.6 %collective-permute-start.6 = (bf16[64,1024]{1,0:T(8,128)(2,1)S(1)}, bf16[64,1024]{1,0:T(8,128)(2,1)S(1)}, u32[]{:S(2)}, u32[]{:S(2)}) collective-permute-start(bf16[64,1024]{1,0:T(8,128)(2,1)S(1)} %get-tuple-element.31), channel_id=1, source_target_pairs={{0,4},{4,0},{8,12},{12,8},{16,20},{20,16},{24,28},{28,24},{1,5},{5... | collective-permute-start | bytes 393224 | tf_op jit(solution)/shard_map/ppermute | solution.py:164
  2.0 0.4 shard_map.91
  2.5 0.1 collective-permute-start
  2.6 3.0 %collective-permute-start.1 = (bf16[32,2048]{1,0:T(8,128)(2,1)S(1)}, bf16[32,2048]{1,0:T(8,128)(2,1)S(1)}, u32[]{:S(2)}, u32[]{:S(2)}) collective-permute-start(bf16[32,2048]{1,0:T(8,128)(2,1)S(1)} %get-tuple-element.24), channel_id=1, source_target_pairs={{0,8},{4,12},{8,0},{12,4},{16,24},{20,28},{24,16},{28,20},{1,9},{5... | collective-permute-start | bytes 393224 | tf_op jit(solution)/shard_map/ppermute | solution.py:164
  5.6 0.0 copy-start
  5.6 0.0 copy-start.1
  5.6 0.0 copy-start.2
  5.7 0.5 shard_map.94
  6.2 1.6 %collective-permute-start.21 = (bf16[256,256]{1,0:T(8,128)(2,1)S(1)}, bf16[256,256]{1,0:T(8,128)(2,1)S(1)}, u32[]{:S(2)}, u32[]{:S(2)}) collective-permute-start(bf16[256,256]{1,0:T(8,128)(2,1)S(1)} %get-tuple-element.37.h0), channel_id=1, source_target_pairs={{0,1},{1,0},{2,3},{3,2},{4,5},{5,4},{6,7},{7,6},{8,9},{9,8},{10,11... | collective-permute-start | bytes 393224 | tf_op jit(solution)/shard_map/ppermute | solution.py:164
  7.7 0.0 collective-permute-done.6
  7.8 3.5 %collective-permute-start.7 = (bf16[64,512]{1,0:T(8,128)(2,1)S(1)}, bf16[64,512]{1,0:T(8,128)(2,1)S(1)}, u32[]{:S(2)}, u32[]{:S(2)}) collective-permute-start(bf16[64,512]{1,0:T(8,128)(2,1)S(1)} %pad_maximum_fusion.3), channel_id=1, source_target_pairs={{0,24},{4,28},{8,16},{12,20},{16,8},{20,12},{24,0},{28,4},{1,25},{... | collective-permute-start | bytes 196616 | tf_op jit(solution)/shard_map/ppermute | solution.py:164
  11.3 0.0 collective-permute-done.b
  11.3 1.6 %collective-permute-start.22 = (bf16[256,256]{1,0:T(8,128)(2,1)S(1)}, bf16[256,256]{1,0:T(8,128)(2,1)S(1)}, u32[]{:S(2)}, u32[]{:S(2)}) collective-permute-start(bf16[256,256]{1,0:T(8,128)(2,1)S(1)} %get-tuple-element.37.h0), channel_id=1, source_target_pairs={{0,2},{1,3},{2,0},{3,1},{4,6},{5,7},{6,4},{7,5},{8,10},{9,11},{10,... | collective-permute-start | bytes 393224 | tf_op jit(solution)/shard_map/ppermute | solution.py:164
  12.9 0.5 collective-permute-start.23
  13.4 2.4 %collective-permute-done.7 = bf16[64,512]{1,0:T(8,128)(2,1)S(1)} collective-permute-done((bf16[64,512]{1,0:T(8,128)(2,1)S(1)}, bf16[64,512]{1,0:T(8,128)(2,1)S(1)}, u32[]{:S(2)}, u32[]{:S(2)}) %collective-permute-start.7) | collective-permute-done | bytes 65568 | tf_op jit(solution)/shard_map/ppermute | solution.py:164
  15.7 0.0 collective-permute-start.8
  15.8 0.0 collective-permute-done.2.d
  15.8 3.0 %collective-permute-start.12 = (bf16[64,512]{1,0:T(8,128)(2,1)S(1)}, bf16[64,512]{1,0:T(8,128)(2,1)S(1)}, u32[]{:S(2)}, u32[]{:S(2)}) collective-permute-start(bf16[64,512]{1,0:T(8,128)(2,1)S(1)} %pad_maximum_fusion.6), channel_id=1, source_target_pairs={{0,16},{4,20},{8,24},{12,28},{16,0},{20,4},{24,8},{28,12},{1,17},{... | collective-permute-start | bytes 196616 | tf_op jit(solution)/shard_map/ppermute | solution.py:164
  18.8 4.3 %collective-permute-done.8 = bf16[64,512]{1,0:T(8,128)(2,1)S(1)} collective-permute-done((bf16[64,512]{1,0:T(8,128)(2,1)S(1)}, bf16[64,512]{1,0:T(8,128)(2,1)S(1)}, u32[]{:S(2)}, u32[]{:S(2)}) %collective-permute-start.8) | collective-permute-done | bytes 65568 | tf_op jit(solution)/shard_map/ppermute | solution.py:164
  23.0 1.0 %collective-permute-start.11 = (bf16[64,512]{1,0:T(8,128)(2,1)S(1)}, bf16[64,512]{1,0:T(8,128)(2,1)S(1)}, u32[]{:S(2)}, u32[]{:S(2)}) collective-permute-start(bf16[64,512]{1,0:T(8,128)(2,1)S(1)} %pad_maximum_fusion.5), channel_id=1, source_target_pairs={{0,24},{4,28},{8,16},{12,20},{16,8},{20,12},{24,0},{28,4},{1,25},{... | collective-permute-start | bytes 196616 | tf_op jit(solution)/shard_map/ppermute | solution.py:164
  24.0 1.6 %collective-permute-start.9 = (bf16[128,512]{1,0:T(8,128)(2,1)S(1)}, bf16[128,512]{1,0:T(8,128)(2,1)S(1)}, u32[]{:S(2)}, u32[]{:S(2)}) collective-permute-start(bf16[128,512]{1,0:T(8,128)(2,1)S(1)} %constant_dynamic-update-slice_fusion.c0), channel_id=1, source_target_pairs={{0,1},{1,0},{2,3},{3,2},{4,5},{5,4},{6,7},{7,6},{8,9},{9,8},{10,11... | collective-permute-start | bytes 393224 | tf_op jit(solution)/shard_map/ppermute | solution.py:164
  25.6 1.5 %collective-permute-start.10 = (bf16[128,512]{1,0:T(8,128)(2,1)S(1)}, bf16[128,512]{1,0:T(8,128)(2,1)S(1)}, u32[]{:S(2)}, u32[]{:S(2)}) collective-permute-start(bf16[128,512]{1,0:T(8,128)(2,1)S(1)} %constant_dynamic-update-slice_fusion.c0), channel_id=1, source_target_pairs={{0,2},{1,3},{2,0},{3,1},{4,6},{5,7},{6,4},{7,5},{8,10},{9,11},{10,... | collective-permute-start | bytes 393224 | tf_op jit(solution)/shard_map/ppermute | solution.py:164
  27.1 1.9 %shard_map.92 = (bf16[128,512]{1,0:T(8,128)(2,1)S(1)}, bf16[128,512]{1,0:T(8,128)(2,1)S(1)}, bf16[128,512]{1,0:T(8,128)(2,1)S(1)}, bf16[128,512]{1,0:T(8,128)(2,1)S(1)}) custom-call(bf16[32,2048]{1,0:T(8,128)(2,1)S(1)} %get-tuple-element.22.a, bf16[32,2048]{1,0:T(8,128)(2,1)S(1)} %collective-permute-done.b, bf16[32,2048]{1,0:T(8,128)(2,1)S(1)} %collective-permute-done.1.c, ...), custom_call_target="tpu_custom_call" | custom-call | tf_op jit(solution)/shard_map/pallas_call | solution.py:235
  29.1 0.5 collective-permute-start.5
  29.6 1.5 %collective-permute-start.4 = (bf16[128,512]{1,0:T(8,128)(2,1)S(1)}, bf16[128,512]{1,0:T(8,128)(2,1)S(1)}, u32[]{:S(2)}, u32[]{:S(2)}) collective-permute-start(bf16[128,512]{1,0:T(8,128)(2,1)S(1)} %get-tuple-element.28), channel_id=1, source_target_pairs={{0,2},{1,3},{2,0},{3,1},{4,6},{5,7},{6,4},{7,5},{8,10},{9,11},{10,... | collective-permute-start | bytes 393224 | tf_op jit(solution)/shard_map/ppermute | solution.py:164
  31.1 1.5 %collective-permute-start.3 = (bf16[128,512]{1,0:T(8,128)(2,1)S(1)}, bf16[128,512]{1,0:T(8,128)(2,1)S(1)}, u32[]{:S(2)}, u32[]{:S(2)}) collective-permute-start(bf16[128,512]{1,0:T(8,128)(2,1)S(1)} %get-tuple-element.27), channel_id=1, source_target_pairs={{0,1},{1,0},{2,3},{3,2},{4,5},{5,4},{6,7},{7,6},{8,9},{9,8},{10,11... | collective-permute-start | bytes 393224 | tf_op jit(solution)/shard_map/ppermute | solution.py:164
  32.6 0.4 shard_map.95.val
  33.1 2.0 %shard_map.93 = (bf16[128,512]{1,0:T(8,128)(2,1)S(1)}, bf16[128,512]{1,0:T(8,128)(2,1)S(1)}, bf16[128,512]{1,0:T(8,128)(2,1)S(1)}, bf16[128,512]{1,0:T(8,128)(2,1)S(1)}) custom-call(bf16[128,512]{1,0:T(8,128)(2,1)S(1)} %constant_dynamic-update-slice_fusion.c0, bf16[128,512]{1,0:T(8,128)(2,1)S(1)} %collective-permute-done.9.c1, ...), custom_call_target="tpu_custom_call" | custom-call | tf_op jit(solution)/shard_map/pallas_call | solution.py:239
  35.1 1.5 %collective-permute-start.15 = (bf16[128,512]{1,0:T(8,128)(2,1)S(1)}, bf16[128,512]{1,0:T(8,128)(2,1)S(1)}, u32[]{:S(2)}, u32[]{:S(2)}) collective-permute-start(bf16[128,512]{1,0:T(8,128)(2,1)S(1)} %get-tuple-element.35), channel_id=1, source_target_pairs={{0,3},{1,2},{2,1},{3,0},{4,7},{5,6},{6,5},{7,4},{8,11},{9,10},{10,... | collective-permute-start | bytes 393224 | tf_op jit(solution)/shard_map/ppermute | solution.py:164
  36.6 1.9 %collective-permute-start.14 = (bf16[128,512]{1,0:T(8,128)(2,1)S(1)}, bf16[128,512]{1,0:T(8,128)(2,1)S(1)}, u32[]{:S(2)}, u32[]{:S(2)}) collective-permute-start(bf16[128,512]{1,0:T(8,128)(2,1)S(1)} %get-tuple-element.34), channel_id=1, source_target_pairs={{0,2},{1,3},{2,0},{3,1},{4,6},{5,7},{6,4},{7,5},{8,10},{9,11},{10,... | collective-permute-start | bytes 393224 | tf_op jit(solution)/shard_map/ppermute | solution.py:164
  38.5 1.4 %collective-permute-start.13 = (bf16[128,512]{1,0:T(8,128)(2,1)S(1)}, bf16[128,512]{1,0:T(8,128)(2,1)S(1)}, u32[]{:S(2)}, u32[]{:S(2)}) collective-permute-start(bf16[128,512]{1,0:T(8,128)(2,1)S(1)} %get-tuple-element.33), channel_id=1, source_target_pairs={{0,1},{1,0},{2,3},{3,2},{4,5},{5,4},{6,7},{7,6},{8,9},{9,8},{10,11... | collective-permute-start | bytes 393224 | tf_op jit(solution)/shard_map/ppermute | solution.py:164
  39.9 0.1 add_convert_fusion.1
  40.0 1.1 %collective-permute-done.15 = bf16[128,512]{1,0:T(8,128)(2,1)S(1)} collective-permute-done((bf16[128,512]{1,0:T(8,128)(2,1)S(1)}, bf16[128,512]{1,0:T(8,128)(2,1)S(1)}, u32[]{:S(2)}, u32[]{:S(2)}) %collective-permute-start.15) | collective-permute-done | bytes 131104 | tf_op jit(solution)/shard_map/ppermute | solution.py:164
  41.1 1.3 %collective-permute-done.14 = bf16[128,512]{1,0:T(8,128)(2,1)S(1)} collective-permute-done((bf16[128,512]{1,0:T(8,128)(2,1)S(1)}, bf16[128,512]{1,0:T(8,128)(2,1)S(1)}, u32[]{:S(2)}, u32[]{:S(2)}) %collective-permute-start.14) | collective-permute-done | bytes 131104 | tf_op jit(solution)/shard_map/ppermute | solution.py:164
  42.4 1.9 %collective-permute-done.13 = bf16[128,512]{1,0:T(8,128)(2,1)S(1)} collective-permute-done((bf16[128,512]{1,0:T(8,128)(2,1)S(1)}, bf16[128,512]{1,0:T(8,128)(2,1)S(1)}, u32[]{:S(2)}, u32[]{:S(2)}) %collective-permute-start.13) | collective-permute-done | bytes 131104 | tf_op jit(solution)/shard_map/ppermute | solution.py:164
  44.3 0.1 add_convert_fusion
  44.4 0.7 %collective-permute-start.17 = (bf16[64,512]{1,0:T(8,128)(2,1)S(1)}, bf16[64,512]{1,0:T(8,128)(2,1)S(1)}, u32[]{:S(2)}, u32[]{:S(2)}) collective-permute-start(bf16[64,512]{1,0:T(8,128)(2,1)S(1)} %get-tuple-element.44), channel_id=1, source_target_pairs={{0,24},{4,28},{8,16},{12,20},{16,8},{20,12},{24,0},{28,4},{1,25},{... | collective-permute-start | bytes 196616 | tf_op jit(solution)/shard_map/ppermute | solution.py:164
  45.1 0.1 collective-permute-start.18
  45.2 0.1 collective-permute-start.20
  45.2 3.7 %collective-permute-start.16 = (bf16[64,512]{1,0:T(8,128)(2,1)S(1)}, bf16[64,512]{1,0:T(8,128)(2,1)S(1)}, u32[]{:S(2)}, u32[]{:S(2)}) collective-permute-start(bf16[64,512]{1,0:T(8,128)(2,1)S(1)} %get-tuple-element.43), channel_id=1, source_target_pairs={{0,16},{4,20},{8,24},{12,28},{16,0},{20,4},{24,8},{28,12},{1,17},{... | collective-permute-start | bytes 196616 | tf_op jit(solution)/shard_map/ppermute | solution.py:164
  48.9 1.6 %collective-permute-done.17 = bf16[64,512]{1,0:T(8,128)(2,1)S(1)} collective-permute-done((bf16[64,512]{1,0:T(8,128)(2,1)S(1)}, bf16[64,512]{1,0:T(8,128)(2,1)S(1)}, u32[]{:S(2)}, u32[]{:S(2)}) %collective-permute-start.17) | collective-permute-done | bytes 65568 | tf_op jit(solution)/shard_map/ppermute | solution.py:164
  50.5 2.5 %collective-permute-done.16 = bf16[64,512]{1,0:T(8,128)(2,1)S(1)} collective-permute-done((bf16[64,512]{1,0:T(8,128)(2,1)S(1)}, bf16[64,512]{1,0:T(8,128)(2,1)S(1)}, u32[]{:S(2)}, u32[]{:S(2)}) %collective-permute-start.16) | collective-permute-done | bytes 65568 | tf_op jit(solution)/shard_map/ppermute | solution.py:164
  53.0 0.2 collective-permute-start.19
  53.2 1.2 %collective-permute-done.19.other = bf16[96,512]{1,0:T(8,128)(2,1)S(1)} collective-permute-done((bf16[96,512]{1,0:T(8,128)(2,1)S(1)}, bf16[96,512]{1,0:T(8,128)(2,1)S(1)}, u32[]{:S(2)}, u32[]{:S(2)}) %collective-permute-start.19) | collective-permute-done | bytes 98336 | tf_op jit(solution)/shard_map/ppermute | solution.py:164
  54.4 1.0 %shard_map.96 = bf16[256,512]{1,0:T(8,128)(2,1)} custom-call(bf16[96,512]{1,0:T(8,128)(2,1)S(1)} %pad_maximum_fusion.1.own, bf16[32,512]{1,0:T(8,128)(2,1)S(1)} %collective-permute-done.18.next_own, bf16[96,512]{1,0:T(8,128)(2,1)S(1)} %collective-permute-done.19.other, bf16[32,512]{1,0:T(8,128)(2,1)S(1)} %collective-permute-done.20.next_other, ...), custom_call_target="tpu_custom_call" | custom-call | tf_op jit(solution)/shard_map/pallas_call | solution.py:263
  (42 shorter events, 0.2 us)
Async XLA Ops:
  0.0 2.0 %copy-start.6 = (s32[8,32]{1,0:T(8,128)S(1)}, s32[8,32]{1,0:T(8,128)}, u32[]{:S(2)}) copy-start(s32[8,32]{1,0:T(8,128)} %chosen.3) | copy-start | bytes 3076
  0.0 2.0 %copy-start.4 = (bf16[256,2048]{1,0:T(8,128)(2,1)S(1)}, bf16[256,2048]{1,0:T(8,128)(2,1)}, u32[]{:S(2)}) copy-start(bf16[256,2048]{1,0:T(8,128)(2,1)} %tokens.5) | copy-start | bytes 3145732
  0.0 2.0 %copy-start.7 = (f32[8,32]{1,0:T(8,128)S(1)}, f32[8,32]{1,0:T(8,128)}, u32[]{:S(2)}) copy-start(f32[8,32]{1,0:T(8,128)} %weights.1) | copy-start | bytes 3076
  1.4 4.2 %copy-start.5 = (bf16[2048,256]{1,0:T(8,128)(2,1)S(1)}, bf16[2048,256]{1,0:T(8,128)(2,1)}, u32[]{:S(2)}) copy-start(bf16[2048,256]{1,0:T(8,128)(2,1)} %w_in.1) | copy-start | bytes 3145732
  1.4 4.2 %copy-start.8 = (bf16[2048]{0:T(1024)(128)(2,1)S(1)}, bf16[2048]{0:T(1024)(128)(2,1)}, u32[]{:S(2)}) copy-start(bf16[2048]{0:T(1024)(128)(2,1)} %w_gate.1) | copy-start | bytes 12292
  1.5 6.3 %collective-permute-start.6 = (bf16[64,1024]{1,0:T(8,128)(2,1)S(1)}, bf16[64,1024]{1,0:T(8,128)(2,1)S(1)}, u32[]{:S(2)}, u32[]{:S(2)}) collective-permute-start(bf16[64,1024]{1,0:T(8,128)(2,1)S(1)} %get-tuple-element.31), channel_id=1, source_target_pairs={{0,4},{4,0},{8,12},{12,8},{16,20},{20,16},{24,28},{28,24},{1,5},{5... | collective-permute-start | bytes 393224 | tf_op jit(solution)/shard_map/ppermute | solution.py:164
  2.5 8.8 %collective-permute-start = (bf16[32,2048]{1,0:T(8,128)(2,1)S(1)}, bf16[32,2048]{1,0:T(8,128)(2,1)S(1)}, u32[]{:S(2)}, u32[]{:S(2)}) collective-permute-start(bf16[32,2048]{1,0:T(8,128)(2,1)S(1)} %get-tuple-element.23), channel_id=1, source_target_pairs={{0,4},{4,0},{8,12},{12,8},{16,20},{20,16},{24,28},{28,24},{1,5},{5... | collective-permute-start | bytes 393224 | tf_op jit(solution)/shard_map/ppermute | solution.py:164
  2.6 10.3 %collective-permute-start.1 = (bf16[32,2048]{1,0:T(8,128)(2,1)S(1)}, bf16[32,2048]{1,0:T(8,128)(2,1)S(1)}, u32[]{:S(2)}, u32[]{:S(2)}) collective-permute-start(bf16[32,2048]{1,0:T(8,128)(2,1)S(1)} %get-tuple-element.24), channel_id=1, source_target_pairs={{0,8},{4,12},{8,0},{12,4},{16,24},{20,28},{24,16},{28,20},{1,9},{5... | collective-permute-start | bytes 393224 | tf_op jit(solution)/shard_map/ppermute | solution.py:164
  5.6 10.2 %collective-permute-start.2 = (bf16[32,2048]{1,0:T(8,128)(2,1)S(1)}, bf16[32,2048]{1,0:T(8,128)(2,1)S(1)}, u32[]{:S(2)}, u32[]{:S(2)}) collective-permute-start(bf16[32,2048]{1,0:T(8,128)(2,1)S(1)} %get-tuple-element.25), channel_id=1, source_target_pairs={{0,12},{4,8},{8,4},{12,0},{16,28},{20,24},{24,20},{28,16},{1,13},{... | collective-permute-start | bytes 393224 | tf_op jit(solution)/shard_map/ppermute | solution.py:164
  5.6 21.5 %copy-start = (bf16[1,2048,1024]{2,1,0:T(8,128)(2,1)S(1)}, bf16[1,2048,1024]{2,1,0:T(8,128)(2,1)}, u32[]{:S(2)}) copy-start(bf16[1,2048,1024]{2,1,0:T(8,128)(2,1)} %param.10) | copy-start | bytes 12582916
  5.6 21.5 %copy-start.1 = (bf16[1,2048,1024]{2,1,0:T(8,128)(2,1)S(1)}, bf16[1,2048,1024]{2,1,0:T(8,128)(2,1)}, u32[]{:S(2)}) copy-start(bf16[1,2048,1024]{2,1,0:T(8,128)(2,1)} %param.11) | copy-start | bytes 12582916
  5.6 21.5 %copy-start.2 = (bf16[1,1024,2048]{2,1,0:T(8,128)(2,1)S(1)}, bf16[1,1024,2048]{2,1,0:T(8,128)(2,1)}, u32[]{:S(2)}) copy-start(bf16[1,1024,2048]{2,1,0:T(8,128)(2,1)} %param.12) | copy-start | bytes 12582916
  6.2 17.9 %collective-permute-start.21 = (bf16[256,256]{1,0:T(8,128)(2,1)S(1)}, bf16[256,256]{1,0:T(8,128)(2,1)S(1)}, u32[]{:S(2)}, u32[]{:S(2)}) collective-permute-start(bf16[256,256]{1,0:T(8,128)(2,1)S(1)} %get-tuple-element.37.h0), channel_id=1, source_target_pairs={{0,1},{1,0},{2,3},{3,2},{4,5},{5,4},{6,7},{7,6},{8,9},{9,8},{10,11... | collective-permute-start | bytes 393224 | tf_op jit(solution)/shard_map/ppermute | solution.py:164
  7.8 8.0 %collective-permute-start.7 = (bf16[64,512]{1,0:T(8,128)(2,1)S(1)}, bf16[64,512]{1,0:T(8,128)(2,1)S(1)}, u32[]{:S(2)}, u32[]{:S(2)}) collective-permute-start(bf16[64,512]{1,0:T(8,128)(2,1)S(1)} %pad_maximum_fusion.3), channel_id=1, source_target_pairs={{0,24},{4,28},{8,16},{12,20},{16,8},{20,12},{24,0},{28,4},{1,25},{... | collective-permute-start | bytes 196616 | tf_op jit(solution)/shard_map/ppermute | solution.py:164
  11.3 14.3 %collective-permute-start.22 = (bf16[256,256]{1,0:T(8,128)(2,1)S(1)}, bf16[256,256]{1,0:T(8,128)(2,1)S(1)}, u32[]{:S(2)}, u32[]{:S(2)}) collective-permute-start(bf16[256,256]{1,0:T(8,128)(2,1)S(1)} %get-tuple-element.37.h0), channel_id=1, source_target_pairs={{0,2},{1,3},{2,0},{3,1},{4,6},{5,7},{6,4},{7,5},{8,10},{9,11},{10,... | collective-permute-start | bytes 393224 | tf_op jit(solution)/shard_map/ppermute | solution.py:164
  12.9 16.1 %collective-permute-start.23 = (bf16[256,256]{1,0:T(8,128)(2,1)S(1)}, bf16[256,256]{1,0:T(8,128)(2,1)S(1)}, u32[]{:S(2)}, u32[]{:S(2)}) collective-permute-start(bf16[256,256]{1,0:T(8,128)(2,1)S(1)} %get-tuple-element.37.h0), channel_id=1, source_target_pairs={{0,3},{1,2},{2,1},{3,0},{4,7},{5,6},{6,5},{7,4},{8,11},{9,10},{10,... | collective-permute-start | bytes 393224 | tf_op jit(solution)/shard_map/ppermute | solution.py:164
  15.7 7.3 %collective-permute-start.8 = (bf16[64,512]{1,0:T(8,128)(2,1)S(1)}, bf16[64,512]{1,0:T(8,128)(2,1)S(1)}, u32[]{:S(2)}, u32[]{:S(2)}) collective-permute-start(bf16[64,512]{1,0:T(8,128)(2,1)S(1)} %pad_maximum_fusion.4), channel_id=1, source_target_pairs={{0,16},{4,20},{8,24},{12,28},{16,0},{20,4},{24,8},{28,12},{1,17},{... | collective-permute-start | bytes 196616 | tf_op jit(solution)/shard_map/ppermute | solution.py:164
  15.8 13.8 %collective-permute-start.12 = (bf16[64,512]{1,0:T(8,128)(2,1)S(1)}, bf16[64,512]{1,0:T(8,128)(2,1)S(1)}, u32[]{:S(2)}, u32[]{:S(2)}) collective-permute-start(bf16[64,512]{1,0:T(8,128)(2,1)S(1)} %pad_maximum_fusion.6), channel_id=1, source_target_pairs={{0,16},{4,20},{8,24},{12,28},{16,0},{20,4},{24,8},{28,12},{1,17},{... | collective-permute-start | bytes 196616 | tf_op jit(solution)/shard_map/ppermute | solution.py:164
  23.0 8.1 %collective-permute-start.11 = (bf16[64,512]{1,0:T(8,128)(2,1)S(1)}, bf16[64,512]{1,0:T(8,128)(2,1)S(1)}, u32[]{:S(2)}, u32[]{:S(2)}) collective-permute-start(bf16[64,512]{1,0:T(8,128)(2,1)S(1)} %pad_maximum_fusion.5), channel_id=1, source_target_pairs={{0,24},{4,28},{8,16},{12,20},{16,8},{20,12},{24,0},{28,4},{1,25},{... | collective-permute-start | bytes 196616 | tf_op jit(solution)/shard_map/ppermute | solution.py:164
  24.0 9.1 %collective-permute-start.9 = (bf16[128,512]{1,0:T(8,128)(2,1)S(1)}, bf16[128,512]{1,0:T(8,128)(2,1)S(1)}, u32[]{:S(2)}, u32[]{:S(2)}) collective-permute-start(bf16[128,512]{1,0:T(8,128)(2,1)S(1)} %constant_dynamic-update-slice_fusion.c0), channel_id=1, source_target_pairs={{0,1},{1,0},{2,3},{3,2},{4,5},{5,4},{6,7},{7,6},{8,9},{9,8},{10,11... | collective-permute-start | bytes 393224 | tf_op jit(solution)/shard_map/ppermute | solution.py:164
  25.6 7.5 %collective-permute-start.10 = (bf16[128,512]{1,0:T(8,128)(2,1)S(1)}, bf16[128,512]{1,0:T(8,128)(2,1)S(1)}, u32[]{:S(2)}, u32[]{:S(2)}) collective-permute-start(bf16[128,512]{1,0:T(8,128)(2,1)S(1)} %constant_dynamic-update-slice_fusion.c0), channel_id=1, source_target_pairs={{0,2},{1,3},{2,0},{3,1},{4,6},{5,7},{6,4},{7,5},{8,10},{9,11},{10,... | collective-permute-start | bytes 393224 | tf_op jit(solution)/shard_map/ppermute | solution.py:164
  27.1 5.5 %copy-start.3 = (bf16[1024,512]{1,0:T(8,128)(2,1)S(1)}, bf16[1024,512]{1,0:T(8,128)(2,1)}, u32[]{:S(2)}) copy-start(bf16[1024,512]{1,0:T(8,128)(2,1)} %w_out.1) | copy-start | bytes 3145732
  29.1 9.4 %collective-permute-start.5 = (bf16[128,512]{1,0:T(8,128)(2,1)S(1)}, bf16[128,512]{1,0:T(8,128)(2,1)S(1)}, u32[]{:S(2)}, u32[]{:S(2)}) collective-permute-start(bf16[128,512]{1,0:T(8,128)(2,1)S(1)} %get-tuple-element.29), channel_id=1, source_target_pairs={{0,3},{1,2},{2,1},{3,0},{4,7},{5,6},{6,5},{7,4},{8,11},{9,10},{10,... | collective-permute-start | bytes 393224 | tf_op jit(solution)/shard_map/ppermute | solution.py:164
  29.6 10.3 %collective-permute-start.4 = (bf16[128,512]{1,0:T(8,128)(2,1)S(1)}, bf16[128,512]{1,0:T(8,128)(2,1)S(1)}, u32[]{:S(2)}, u32[]{:S(2)}) collective-permute-start(bf16[128,512]{1,0:T(8,128)(2,1)S(1)} %get-tuple-element.28), channel_id=1, source_target_pairs={{0,2},{1,3},{2,0},{3,1},{4,6},{5,7},{6,4},{7,5},{8,10},{9,11},{10,... | collective-permute-start | bytes 393224 | tf_op jit(solution)/shard_map/ppermute | solution.py:164
  31.1 8.8 %collective-permute-start.3 = (bf16[128,512]{1,0:T(8,128)(2,1)S(1)}, bf16[128,512]{1,0:T(8,128)(2,1)S(1)}, u32[]{:S(2)}, u32[]{:S(2)}) collective-permute-start(bf16[128,512]{1,0:T(8,128)(2,1)S(1)} %get-tuple-element.27), channel_id=1, source_target_pairs={{0,1},{1,0},{2,3},{3,2},{4,5},{5,4},{6,7},{7,6},{8,9},{9,8},{10,11... | collective-permute-start | bytes 393224 | tf_op jit(solution)/shard_map/ppermute | solution.py:164
  35.1 6.0 %collective-permute-start.15 = (bf16[128,512]{1,0:T(8,128)(2,1)S(1)}, bf16[128,512]{1,0:T(8,128)(2,1)S(1)}, u32[]{:S(2)}, u32[]{:S(2)}) collective-permute-start(bf16[128,512]{1,0:T(8,128)(2,1)S(1)} %get-tuple-element.35), channel_id=1, source_target_pairs={{0,3},{1,2},{2,1},{3,0},{4,7},{5,6},{6,5},{7,4},{8,11},{9,10},{10,... | collective-permute-start | bytes 393224 | tf_op jit(solution)/shard_map/ppermute | solution.py:164
  36.6 5.8 %collective-permute-start.14 = (bf16[128,512]{1,0:T(8,128)(2,1)S(1)}, bf16[128,512]{1,0:T(8,128)(2,1)S(1)}, u32[]{:S(2)}, u32[]{:S(2)}) collective-permute-start(bf16[128,512]{1,0:T(8,128)(2,1)S(1)} %get-tuple-element.34), channel_id=1, source_target_pairs={{0,2},{1,3},{2,0},{3,1},{4,6},{5,7},{6,4},{7,5},{8,10},{9,11},{10,... | collective-permute-start | bytes 393224 | tf_op jit(solution)/shard_map/ppermute | solution.py:164
  38.5 5.8 %collective-permute-start.13 = (bf16[128,512]{1,0:T(8,128)(2,1)S(1)}, bf16[128,512]{1,0:T(8,128)(2,1)S(1)}, u32[]{:S(2)}, u32[]{:S(2)}) collective-permute-start(bf16[128,512]{1,0:T(8,128)(2,1)S(1)} %get-tuple-element.33), channel_id=1, source_target_pairs={{0,1},{1,0},{2,3},{3,2},{4,5},{5,4},{6,7},{7,6},{8,9},{9,8},{10,11... | collective-permute-start | bytes 393224 | tf_op jit(solution)/shard_map/ppermute | solution.py:164
  44.4 6.1 %collective-permute-start.17 = (bf16[64,512]{1,0:T(8,128)(2,1)S(1)}, bf16[64,512]{1,0:T(8,128)(2,1)S(1)}, u32[]{:S(2)}, u32[]{:S(2)}) collective-permute-start(bf16[64,512]{1,0:T(8,128)(2,1)S(1)} %get-tuple-element.44), channel_id=1, source_target_pairs={{0,24},{4,28},{8,16},{12,20},{16,8},{20,12},{24,0},{28,4},{1,25},{... | collective-permute-start | bytes 196616 | tf_op jit(solution)/shard_map/ppermute | solution.py:164
  45.1 8.1 %collective-permute-start.18 = (bf16[32,512]{1,0:T(8,128)(2,1)S(1)}, bf16[32,512]{1,0:T(8,128)(2,1)S(1)}, u32[]{:S(2)}, u32[]{:S(2)}) collective-permute-start(bf16[32,512]{1,0:T(8,128)(2,1)S(1)} %get-tuple-element.41), channel_id=1, source_target_pairs={{0,8},{4,12},{8,0},{12,4},{16,24},{20,28},{24,16},{28,20},{1,9},{5... | collective-permute-start | bytes 98312 | tf_op jit(solution)/shard_map/ppermute | solution.py:164
  45.2 8.1 %collective-permute-start.20 = (bf16[32,512]{1,0:T(8,128)(2,1)S(1)}, bf16[32,512]{1,0:T(8,128)(2,1)S(1)}, u32[]{:S(2)}, u32[]{:S(2)}) collective-permute-start(bf16[32,512]{1,0:T(8,128)(2,1)S(1)} %get-tuple-element.39), channel_id=1, source_target_pairs={{0,12},{4,8},{8,4},{12,0},{16,28},{20,24},{24,20},{28,16},{1,13},{... | collective-permute-start | bytes 98312 | tf_op jit(solution)/shard_map/ppermute | solution.py:164
  45.2 7.8 %collective-permute-start.16 = (bf16[64,512]{1,0:T(8,128)(2,1)S(1)}, bf16[64,512]{1,0:T(8,128)(2,1)S(1)}, u32[]{:S(2)}, u32[]{:S(2)}) collective-permute-start(bf16[64,512]{1,0:T(8,128)(2,1)S(1)} %get-tuple-element.43), channel_id=1, source_target_pairs={{0,16},{4,20},{8,24},{12,28},{16,0},{20,4},{24,8},{28,12},{1,17},{... | collective-permute-start | bytes 196616 | tf_op jit(solution)/shard_map/ppermute | solution.py:164
  53.0 1.4 %collective-permute-start.19 = (bf16[96,512]{1,0:T(8,128)(2,1)S(1)}, bf16[96,512]{1,0:T(8,128)(2,1)S(1)}, u32[]{:S(2)}, u32[]{:S(2)}) collective-permute-start(bf16[96,512]{1,0:T(8,128)(2,1)S(1)} %pad_maximum_fusion.2), channel_id=1, source_target_pairs={{0,4},{4,0},{8,12},{12,8},{16,20},{20,16},{24,28},{28,24},{1,5},{5... | collective-permute-start | bytes 294920 | tf_op jit(solution)/shard_map/ppermute | solution.py:164
